TPU v7x, 32 devices: a whole 2x2x4 slice. The times are simulated.
32 devices in a mesh: sp: 8 (over z, x), tp: 4 (over y, core).
Axes of the slice: x: 2, y: 2, z: 4, core: 2. Of those that a mesh axis runs over, the one named last changes fastest.
Arguments:
- queries: bfloat16 [4096, 3072], P('sp', 'tp'), may hold values from -6 to 6
- latent: bfloat16 [4096, 1024], P('sp'), may hold values from -6 to 6
- rope_key: bfloat16 [4096, 64], P('sp'), may hold values from -6 to 6
- key_weight: bfloat16 [1024, 2048], P(None, 'tp'), as said below
- value_weight: bfloat16 [1024, 2048], P(None, 'tp'), as said below
- log_sums: float32 [16, 4096], P('tp', 'sp'), as said below
- attn_out: bfloat16 [4096, 2048], P('sp', 'tp'), as said below
- out_grad: bfloat16 [4096, 2048], P('sp', 'tp'), may hold values from -6 to 6
Outputs:
- d_queries: bfloat16 [4096, 3072], P('sp', 'tp')
- d_latent: float32 [4096, 1024], P('sp')
- d_rope: float32 [4096, 64], P('sp')
- d_value_weight: float32 [1024, 2048], P('sp', 'tp')
Inputs may be any that keep to these rules, and one draw needn't show every extreme that they name: `key_weight`: independent entries of order one multiplied by 1024^(-1/2). `value_weight`: independent entries of order one multiplied by 1024^(-1/2). log_sums[h, i] is the logarithm of the sum over j <= i of exp(scores[h, i, j]) of the forward pass. attn_out is the forward pass output: head h of row i is the sum over j <= i of exp(scores - log_sums) rounded to bfloat16, times head h of values row j, rounded to bfloat16.
All inputs are finite; a program needn't handle non-finite values.
Results may differ from a plain program's by a relative error of at most 0.018.
Values may be sent and summed in bfloat16 or wider, within the bound.
A program may use at most 192 MiB of HBM per device.

v0:
```python
import functools

import jax
import jax.numpy as jnp
from jax import lax
from jax.experimental import pallas as pl
from jax.experimental.pallas import tpu as pltpu
from jax.sharding import PartitionSpec as P

NOPE = 128
ROPE = 64
VDIM = 128
WIDE = 256
LOG2E = 1.4426950408889634
BF16 = jnp.bfloat16
F32 = jnp.float32


def dot_nn(a, b):
    return lax.dot_general(a, b, (((1,), (0,)), ((), ())), preferred_element_type=F32)


def dot_nt(a, b):
    return lax.dot_general(a, b, (((1,), (1,)), ((), ())), preferred_element_type=F32)


def attn_kernel(
    heads,
    latent_dim,
    mine_ref,
    q_ref,
    g_ref,
    lse_ref,
    delta_ref,
    lat_ref,
    wk_ref,
    wv_ref,
    dq_ref,
    dlat_ref,
    dvw_ref,
    q_s,
    qt_s,
    gt_s,
    dqt_s,
    kc_s,
    kct_s,
    v_s,
    dk_s,
    dv_s,
):
    j = pl.program_id(0)
    mine = mine_ref[0]
    rows = q_ref.shape[0]
    width = NOPE + ROPE
    scale = width ** (-0.5)

    @pl.when(j == 0)
    def _():
        for h in range(heads):
            qh = jnp.concatenate(
                [q_ref[:, h * width : (h + 1) * width], jnp.zeros((rows, WIDE - width), BF16)],
                axis=1,
            )
            q_s[h] = qh
            qt_s[h] = qh.T
            gt_s[h] = g_ref[:, h * VDIM : (h + 1) * VDIM].T
        dqt_s[...] = jnp.zeros_like(dqt_s)
        dvw_ref[...] = jnp.zeros_like(dvw_ref)

    @pl.when(j > mine)
    def _():
        dlat_ref[...] = jnp.zeros_like(dlat_ref)

    @pl.when(j <= mine)
    def _():
        lat = lat_ref[:, :latent_dim]
        rope = lat_ref[:, latent_dim:]
        keys = dot_nn(lat, wk_ref[...]).astype(BF16)
        v_s[...] = dot_nn(lat, wv_ref[...]).astype(BF16)
        for h in range(heads):
            kc = jnp.concatenate([keys[:, h * NOPE : (h + 1) * NOPE], rope], axis=1)
            kc_s[h] = kc
            kct_s[h] = kc.T
        rope_sum = jnp.zeros((rows, WIDE - NOPE), F32)
        k_pos = lax.broadcasted_iota(jnp.int32, (rows, rows), 0)
        q_pos = lax.broadcasted_iota(jnp.int32, (rows, rows), 1)
        causal = k_pos - q_pos <= (mine - j) * rows
        for h in range(heads):
            s = dot_nn(kc_s[h], qt_s[h])
            z = s * (scale * LOG2E) - lse_ref[h : h + 1, :] * LOG2E
            p = jnp.exp2(jnp.where(causal, z, -1e30))
            dp = dot_nn(v_s[:, h * VDIM : (h + 1) * VDIM], gt_s[h])
            ds = (p * (dp - delta_ref[h : h + 1, :])).astype(BF16)
            dv_s[:, h * VDIM : (h + 1) * VDIM] = dot_nn(
                p.astype(BF16), g_ref[:, h * VDIM : (h + 1) * VDIM]
            ).astype(BF16)
            dk = scale * dot_nn(ds, q_s[h])
            dk_s[:, h * NOPE : (h + 1) * NOPE] = dk[:, :NOPE].astype(BF16)
            rope_sum = rope_sum + dk[:, NOPE:]
            dqt_s[h] += dot_nn(kct_s[h], ds)
        dlat = dot_nt(dk_s[...], wk_ref[...]) + dot_nt(dv_s[...], wv_ref[...])
        dlat_ref[:, :latent_dim] = dlat.astype(BF16)
        dlat_ref[:, latent_dim:] = rope_sum.astype(BF16)
        dvw_ref[...] += dot_nn(lat.T, dv_s[...])

    @pl.when(j == pl.num_programs(0) - 1)
    def _():
        for h in range(heads):
            dq_ref[:, h * width : (h + 1) * width] = (
                (scale * dqt_s[h]).T[:, :width].astype(BF16)
            )


def attn_backward(mine, queries, out_grad, lse, delta, lat_all, key_weight, value_weight):
    rows = queries.shape[0]
    latent_dim = key_weight.shape[0]
    heads = key_weight.shape[1] // NOPE
    blocks = lat_all.shape[0] // rows
    packed = lat_all.shape[1]

    def whole(j, m):
        return (0, 0)

    return pl.pallas_call(
        functools.partial(attn_kernel, heads, latent_dim),
        grid_spec=pltpu.PrefetchScalarGridSpec(
            num_scalar_prefetch=1,
            grid=(blocks,),
            in_specs=[
                pl.BlockSpec(queries.shape, whole),
                pl.BlockSpec(out_grad.shape, whole),
                pl.BlockSpec(lse.shape, whole),
                pl.BlockSpec(delta.shape, whole),
                pl.BlockSpec((rows, packed), lambda j, m: (jnp.minimum(j, m[0]), 0)),
                pl.BlockSpec(key_weight.shape, whole),
                pl.BlockSpec(value_weight.shape, whole),
            ],
            out_specs=[
                pl.BlockSpec(queries.shape, whole),
                pl.BlockSpec((rows, packed), lambda j, m: (j, 0)),
                pl.BlockSpec(value_weight.shape, whole),
            ],
            scratch_shapes=[
                pltpu.VMEM((heads, rows, WIDE), BF16),
                pltpu.VMEM((heads, WIDE, rows), BF16),
                pltpu.VMEM((heads, VDIM, rows), BF16),
                pltpu.VMEM((heads, WIDE, rows), F32),
                pltpu.VMEM((heads, rows, WIDE), BF16),
                pltpu.VMEM((heads, WIDE, rows), BF16),
                pltpu.VMEM((rows, heads * VDIM), BF16),
                pltpu.VMEM((rows, heads * NOPE), BF16),
                pltpu.VMEM((rows, heads * VDIM), BF16),
            ],
        ),
        out_shape=[
            jax.ShapeDtypeStruct(queries.shape, BF16),
            jax.ShapeDtypeStruct(lat_all.shape, BF16),
            jax.ShapeDtypeStruct(value_weight.shape, F32),
        ],
        compiler_params=pltpu.CompilerParams(
            dimension_semantics=("arbitrary",), vmem_limit_bytes=60 * 1024 * 1024
        ),
    )(mine, queries, out_grad, lse, delta, lat_all, key_weight, value_weight)


def per_device(queries, latent, rope_key, key_weight, value_weight, log_sums, attn_out, out_grad):
    rows, latent_dim = latent.shape
    heads = key_weight.shape[1] // NOPE
    tp = lax.axis_size("tp")
    mine = lax.axis_index("sp").astype(jnp.int32).reshape((1,))
    row_terms = jnp.sum(
        attn_out.reshape(rows, heads, VDIM).astype(F32)
        * out_grad.reshape(rows, heads, VDIM).astype(F32),
        axis=2,
    ).T
    part = rows // tp
    start = lax.axis_index("tp") * part
    lat_piece = lax.dynamic_slice_in_dim(latent, start, part, 0)
    rope_piece = lax.dynamic_slice_in_dim(rope_key, start, part, 0)
    piece = jnp.concatenate(
        [lat_piece, rope_piece, jnp.zeros((part, WIDE - NOPE - ROPE), BF16)], axis=1
    )
    lat_all = lax.all_gather(piece, ("sp", "tp"), axis=0, tiled=True)
    d_queries, dlat, dvw = attn_backward(
        mine, queries, out_grad, log_sums, row_terms, lat_all, key_weight, value_weight
    )
    dlat_piece = lax.psum_scatter(dlat, ("sp", "tp"), scatter_dimension=0, tiled=True)
    sp = lax.axis_size("sp")
    dvw_parts = lax.all_to_all(dvw.astype(BF16), "sp", 0, 0, tiled=True)
    d_value_weight = jnp.sum(
        dvw_parts.reshape(sp, latent_dim // sp, dvw.shape[1]).astype(F32), axis=0
    )
    dlat_own = lax.all_gather(dlat_piece, "tp", axis=0, tiled=True)
    d_latent = dlat_own[:, :latent_dim].astype(F32)
    d_rope = dlat_own[:, latent_dim : latent_dim + ROPE].astype(F32)
    return (d_queries, d_latent, d_rope, d_value_weight)


def solution(mesh):
    placed = (
        P("sp", "tp"),
        P("sp", None),
        P("sp", None),
        P(None, "tp"),
        P(None, "tp"),
        P("tp", "sp"),
        P("sp", "tp"),
        P("sp", "tp"),
    )
    return jax.shard_map(
        per_device,
        mesh=mesh,
        in_specs=placed,
        out_specs=(P("sp", "tp"), P("sp", None), P("sp", None), P("sp", "tp")),
        check_vma=False,
    )
```

profile of v0, /device:TPU:0, one launch (start us, length us, event | category | flops | bytes accessed | tf_op | source)
XLA Modules:
  0.0 312.5 jit_solution(7623646440613211574)
XLA Ops:
  7.2 0.0 all-gather.3.cloned.1.call-start
  7.2 0.8 constant_dynamic-slice_fusion
  8.0 0.1 copy.17
  8.2 0.3 copy-done
  8.4 0.8 concatenate.3
  9.3 0.0 all-gather.3.cloned.1.call-update
  9.3 0.0 reduce-scatter.2.cloned.1.call-start
  9.3 1.3 convert_multiply_fusion
  10.7 0.4 mul.10
  11.1 0.6 reduce_sum.18
  11.7 0.7 copy.14
  12.4 83.3 %all-gather.3.cloned.1.call-done.lat_ref = bf16[4096,1152]{1,0:T(8,128)(2,1)} async-done(((bf16[128,1152]{1,0:T(8,128)(2,1)}), bf16[4096,1152]{1,0:T(8,128)(2,1)}) %all-gather.3.cloned.1.call-update) | async-done | bytes 9437200 | tf_op jit(solution)/shard_map/all_gather | solution.py:183
  95.7 15.2 %shard_map.111 = (bf16[512,768]{1,0:T(8,128)(2,1)}, bf16[4096,1152]{1,0:T(8,128)(2,1)}, f32[1024,512]{1,0:T(8,128)}) custom-call(s32[1]{0:T(128)} %bitcast.mine_ref, bf16[512,768]{1,0:T(8,128)(2,1)} %q_ref.1, bf16[512,512]{1,0:T(8,128)(2,1)} %g_ref.1, f32[4,512]{1,0:T(4,128)} %lse_ref.1, f32[4,512]{1,0:T(4,128)} %bitcast.3, ...), custom_call_target="tpu_custom_call" | custom-call | tf_op jit(solution)/shard_map/pallas_call | solution.py:124
  110.9 0.0 reduce-scatter.2.cloned.1.call-update
  110.9 1.6 copy-done.1
  112.5 1.1 convert_element_type.24
  113.6 41.7 %all-to-all-start = ((bf16[8,128,512]{2,1,0:T(8,128)(2,1)}), bf16[8,128,512]{2,1,0:T(8,128)(2,1)S(1)}, u32[]{:S(2)}, u32[]{:S(2)}) async-start(bf16[8,128,512]{2,1,0:T(8,128)(2,1)} %bitcast.2), calls=%async_computation.1 | async-start | bytes 2097152 | tf_op jit(solution)/shard_map/all_to_all | solution.py:189
  155.3 0.0 all-gather.5.cloned.1.call-start
  155.3 128.2 %reduce-scatter.2.cloned.1.call-done = bf16[128,1152]{1,0:T(8,128)(2,1)} async-done(((bf16[4096,1152]{1,0:T(8,128)(2,1)}), bf16[128,1152]{1,0:T(8,128)(2,1)}) %reduce-scatter.2.cloned.1.call-update) | async-done | bytes 294928 | tf_op jit(solution)/shard_map/reduce_scatter | solution.py:187
  283.5 0.8 convert_reduce_fusion
  284.4 17.1 %all-gather.5.cloned.1.call-done = bf16[512,1152]{1,0:T(8,128)(2,1)} async-done(((bf16[128,1152]{1,0:T(8,128)(2,1)}), bf16[512,1152]{1,0:T(8,128)(2,1)}) %all-gather.5.cloned.1.call-update) | async-done | bytes 1179664 | tf_op jit(solution)/shard_map/all_gather | solution.py:193
  301.5 0.9 slice_convert_fusion.1
  302.4 0.8 copy.16
  303.2 2.8 slice_convert_fusion
  (6 shorter events, 0.1 us)
Async XLA Ops:
  7.2 1.2 copy-start
  7.2 88.5 %all-gather.3.cloned.1.call-start = ((), (), s32[]{:S(2)}) async-start(), calls=%async_computation.2 | async-start | bytes 9732096 | tf_op jit(solution)/shard_map/all_gather | solution.py:183
  9.3 274.2 %reduce-scatter.2.cloned.1.call-start = ((), (), s32[]{:S(2)}) async-start(), calls=%async_computation.3 | async-start | bytes 9732096 | tf_op jit(solution)/shard_map/reduce_scatter | solution.py:187
  110.9 1.6 copy-start.1
  113.6 169.9 %all-to-all-start = ((bf16[8,128,512]{2,1,0:T(8,128)(2,1)}), bf16[8,128,512]{2,1,0:T(8,128)(2,1)S(1)}, u32[]{:S(2)}, u32[]{:S(2)}) async-start(bf16[8,128,512]{2,1,0:T(8,128)(2,1)} %bitcast.2), calls=%async_computation.1 | async-start | bytes 2097152 | tf_op jit(solution)/shard_map/all_to_all | solution.py:189
  155.3 146.2 %all-gather.5.cloned.1.call-start = ((), (), s32[]{:S(2)}) async-start(), calls=%async_computation.4 | async-start | bytes 1474560 | tf_op jit(solution)/shard_map/all_gather | solution.py:193
Sparse Core Ops, SparseCore 0:
  11.5 84.1 all-gather.2
  111.0 172.4 reduce-scatter.1
  285.1 16.3 all-gather.4
where the time goes:
time: 313 us
  waiting for transfers between devices  229 us (73%)
  starting transfers between devices  41.8 us (13%)
  Pallas kernels  15.2 us (5%)
  between operations  13.8 us (4%)
  other arithmetic  7.62 us (2%)
  local copies, waits for them, and re-layouts  5.43 us (2%)
    reduce_scatter x1, waiting for transfers between devices, per_device(): lax.psum_scatter(dlat, ('sp', 'tp'), scatter_dimension=0, tiled=True)  128 us
    all_gather x1, waiting for transfers between devices, per_device(): lat_all = lax.all_gather(piece, ('sp', 'tp'), axis=0, tiled=True)  83.3 us
    all_to_all x1, starting transfers between devices, per_device(): dvw_parts = lax.all_to_all(dvw.astype(BF16), 'sp', 0, 0, tiled=True)  41.7 us
    all_gather x1, waiting for transfers between devices, per_device(): dlat_own = lax.all_gather(dlat_piece, 'tp', axis=0, tiled=True)  17.1 us
    pallas_call x1, Pallas kernels, attn_backward(): pl.pallas_call(functools.partial(attn_kernel, heads, latent_dim), grid_sp...  15.2 us
  transfers between devices with their start and end apart: 4, of which 3 were waited for; matrix products, arithmetic and copies ran while one was open for 2% of the time, Pallas kernels for 0%

commit v1 on v0

v1 whole, which is shorter than its diff:
```python
import functools

import jax
import jax.numpy as jnp
from jax import lax
from jax.experimental import pallas as pl
from jax.experimental.pallas import tpu as pltpu
from jax.sharding import PartitionSpec as P

NOPE = 128
ROPE = 64
VDIM = 128
WIDE = 256
LOG2E = 1.4426950408889634
BF16 = jnp.bfloat16
F32 = jnp.float32
MESH = pl.DeviceIdType.MESH


def dot_nn(a, b):
    return lax.dot_general(a, b, (((1,), (0,)), ((), ())), preferred_element_type=F32)


def dot_nt(a, b):
    return lax.dot_general(a, b, (((1,), (1,)), ((), ())), preferred_element_type=F32)


def fused_kernel(
    ns,
    tp,
    heads,
    latent_dim,
    q_hbm,
    g_hbm,
    ao_hbm,
    lse_ref,
    latp_hbm,
    wk_hbm,
    wv_hbm,
    dq_ref,
    dlat_hbm,
    dvw_ref,
    q_v,
    g_v,
    ao_v,
    wk_v,
    wv_v,
    qs_s,
    qt_s,
    gt_s,
    dqt_s,
    delta_s,
    kc_s,
    kct_s,
    v_s,
    dk_s,
    dv_s,
    dvw_acc,
    dvw_b,
    dvw_rx,
    lat_all,
    crx,
    yrx,
    orx,
    own_acc,
    fin,
    ld,
    zr,
    zs,
    ds_,
    xr,
    xs,
    car,
    cas,
    cbr,
    cbs,
    r1r,
    r1s,
    yr,
    ys,
    orr,
    ors,
    dvr,
    dvs,
    agr,
    ags,
    acr,
    acs,
):
    i = lax.axis_index("sp")
    t = lax.axis_index("tp")
    ny = tp // 2
    nz = ns // 2
    z, x = i // 2, i % 2
    y, c = t // 2, t % 2
    rows, width = q_v.shape[0], NOPE + ROPE
    half, quart, piece = rows // 2, rows // 4, rows // tp
    scale = width ** (-0.5)
    lrows = latent_dim // ns

    first = 1 - x
    last = 2 * z + 1

    def block_of(n):
        return last - n

    my_half = pl.multiple_of(c * half, half)
    peer_half = pl.multiple_of((1 - c) * half, half)
    my_q = pl.multiple_of(c * half + x * quart, quart)
    other_q = pl.multiple_of(c * half + (1 - x) * quart, quart)
    core_peer = {"sp": i, "tp": y * 2 + 1 - c}
    x_peer = {"sp": 2 * z + 1 - x, "tp": t}

    def remote(src, dst, ssem, rsem, dev):
        return pltpu.make_async_remote_copy(
            src_ref=src, dst_ref=dst, send_sem=ssem, recv_sem=rsem, device_id=dev, device_id_type=MESH
        )

    def lat_rows(j, at, size):
        return lat_all.at[j, pl.ds(at, size)]

    own_cp = pltpu.make_async_copy(latp_hbm, lat_all.at[i], ld.at[0])
    own_cp.start()
    loads = [
        pltpu.make_async_copy(s, d, ld.at[k + 1])
        for k, (s, d) in enumerate(
            ((wk_hbm, wk_v), (wv_hbm, wv_v), (q_hbm, q_v), (g_hbm, g_v), (ao_hbm, ao_v))
        )
    ]
    for cp in loads:
        cp.start()

    barrier = pltpu.get_barrier_semaphore()
    for d in range(1, ns):
        pl.semaphore_signal(
            barrier, inc=1, device_id={"sp": (i + d) % ns, "tp": t}, device_id_type=MESH
        )
    for d in range(1, tp):
        pl.semaphore_signal(
            barrier, inc=1, device_id={"sp": i, "tp": (t + d) % tp}, device_id_type=MESH
        )
    pl.semaphore_wait(barrier, ns - 1 + tp - 1)
    own_cp.wait()

    def z_copy(j):
        return remote(
            lat_rows(j, my_q, quart), lat_rows(j, my_q, quart), zs.at[j], zr.at[j],
            {"sp": lax.min(i + 2, ns - 1), "tp": t},
        )

    def diag_copy():
        return remote(
            lat_rows(i, other_q, quart), lat_rows(i, other_q, quart), ds_.at[0], zr.at[i],
            {"sp": lax.min(2 * z + 3 - x, ns - 1), "tp": t},
        )

    def x_copy(j):
        return remote(
            lat_rows(j, my_q, quart), lat_rows(j, my_q, quart), xs.at[j], xr.at[j], x_peer
        )

    def x_wait(j):
        return remote(
            lat_rows(j, other_q, quart), lat_rows(j, other_q, quart), xs.at[j], xr.at[j], x_peer
        )

    def xh_copy(j):
        return remote(
            lat_rows(j, my_half, half), lat_rows(j, my_half, half), xs.at[j], xr.at[j], x_peer
        )

    def ca_copy(j):
        return remote(
            lat_rows(j, my_q, quart), lat_rows(j, my_q, quart), cas.at[j], car.at[j], core_peer
        )

    def cb_copy(j):
        return remote(
            lat_rows(j, other_q, quart), lat_rows(j, other_q, quart), cbs.at[j], cbr.at[j], core_peer
        )

    def ch_copy(j):
        return remote(
            lat_rows(j, my_half, half), lat_rows(j, my_half, half), cbs.at[j], cbr.at[j], core_peer
        )

    has_next = z + 1 < nz

    @pl.when(has_next)
    def _():
        z_copy(i).start()
        diag_copy().start()

    @pl.when(x == 0)
    def _():
        xh_copy(i).start()

    def stage_a(n):
        @pl.when(jnp.logical_and(n >= 2, n <= last))
        def _():
            j = block_of(n)
            z_copy(j).wait_recv()
            x_copy(j).start()
            ca_copy(j).start()

            @pl.when(has_next)
            def _():
                z_copy(j).start()

    def stage_b(n):
        j = block_of(n)

        @pl.when(jnp.logical_and(n == 1, x == 1))
        def _():
            xh_copy(j).wait_recv()
            ch_copy(j).start()

        @pl.when(jnp.logical_and(n >= 2, n <= last))
        def _():
            x_wait(j).wait_recv()
            cb_copy(j).start()

    def stage_c(n):
        j = block_of(n)

        @pl.when(jnp.logical_and(n == 1, x == 1))
        def _():
            ch_copy(j).wait_recv()

        @pl.when(n >= 2)
        def _():
            ca_copy(j).wait_recv()
            cb_copy(j).wait_recv()

    def sends_done(n):
        j = block_of(n)

        @pl.when(n == first)
        def _():
            @pl.when(has_next)
            def _():
                z_copy(i).wait_send()
                diag_copy().wait_send()

            @pl.when(x == 0)
            def _():
                xh_copy(i).wait_send()

        @pl.when(jnp.logical_and(n == 1, x == 1))
        def _():
            ch_copy(j).wait_send()

        @pl.when(n >= 2)
        def _():
            x_copy(j).wait_send()
            ca_copy(j).wait_send()
            cb_copy(j).wait_send()

            @pl.when(has_next)
            def _():
                z_copy(j).wait_send()

    def r1_copy(j):
        return remote(
            lat_rows(j + 1, peer_half, half), crx.at[j], r1s.at[j], r1r.at[j], core_peer
        )

    def y_copy(j, d):
        yy = (y + d) % ny
        at = pl.multiple_of(c * half + yy * piece, piece)
        return remote(
            lat_rows(j + 1, at, piece), yrx.at[j, d - 1], ys.at[j, d - 1], yr.at[j, d - 1],
            {"sp": i, "tp": yy * 2 + c},
        )

    my_piece = pl.multiple_of(c * half + y * piece, piece)

    def o_copy(j):
        return remote(
            lat_rows(j + 1, my_piece, piece), orx.at[i], ors.at[j], orr.at[i], {"sp": j, "tp": t}
        )

    def o_wait(src):
        return remote(
            lat_rows(i + 1, my_piece, piece), orx.at[src], ors.at[i], orr.at[src], {"sp": src, "tp": t}
        )

    def stage_r2(n):
        j = block_of(n)
        r1_copy(j).wait_recv()
        mine = lat_all[j + 1, pl.ds(my_half, half), :].astype(F32)
        lat_all[j + 1, pl.ds(my_half, half), :] = (mine + crx[j].astype(F32)).astype(BF16)
        for d in range(1, ny):
            y_copy(j, d).start()

    def stage_r3(n):
        j = block_of(n)
        total = lat_all[j + 1, pl.ds(my_piece, piece), :].astype(F32)
        for d in range(1, ny):
            y_copy(j, d).wait_recv()
            total = total + yrx[j, d - 1].astype(F32)
        for d in range(1, ny):
            y_copy(j, d).wait_send()
        r1_copy(j).wait_send()

        @pl.when(n == first)
        def _():
            own_acc[...] = total

        @pl.when(n > first)
        def _():
            lat_all[j + 1, pl.ds(my_piece, piece), :] = total.astype(BF16)
            o_copy(j).start()

    for cp in loads:
        cp.wait()
    for h in range(heads):
        qh = jnp.concatenate(
            [q_v[:, h * width : (h + 1) * width], jnp.zeros((rows, WIDE - width), BF16)], axis=1
        )
        qs_s[h] = qh
        qt_s[h] = qh.T
        gt = g_v[:, h * VDIM : (h + 1) * VDIM].T
        gt_s[h] = gt
        at = ao_v[:, h * VDIM : (h + 1) * VDIM].T
        delta_s[h : h + 1, :] = jnp.sum(gt.astype(F32) * at.astype(F32), axis=0, keepdims=True)
    dqt_s[...] = jnp.zeros_like(dqt_s)
    dvw_acc[...] = jnp.zeros_like(dvw_acc)

    def slot(n, carry):
        j = block_of(n)
        stage_c(n)
        rope = lat_all[j, :, latent_dim:]
        keys = dot_nn(lat_all[j, :, :latent_dim], wk_v[...]).astype(BF16)
        v_s[...] = dot_nn(lat_all[j, :, :latent_dim], wv_v[...]).astype(BF16)
        for h in range(heads):
            kc = jnp.concatenate([keys[:, h * NOPE : (h + 1) * NOPE], rope], axis=1)
            kc_s[h] = kc
            kct_s[h] = kc.T
        rope_sum = jnp.zeros((rows, WIDE - NOPE), F32)
        k_pos = lax.broadcasted_iota(jnp.int32, (rows, rows), 0)
        q_pos = lax.broadcasted_iota(jnp.int32, (rows, rows), 1)
        causal = k_pos - q_pos <= (i - j) * rows
        for h in range(heads):
            s = dot_nn(kc_s[h], qt_s[h])
            zz = s * (scale * LOG2E) - lse_ref[h : h + 1, :] * LOG2E
            p = jnp.exp2(jnp.where(causal, zz, -1e30))
            dp = dot_nn(v_s[:, h * VDIM : (h + 1) * VDIM], gt_s[h])
            ds = (p * (dp - delta_s[h : h + 1, :])).astype(BF16)
            dv_s[:, h * VDIM : (h + 1) * VDIM] = dot_nn(
                p.astype(BF16), g_v[:, h * VDIM : (h + 1) * VDIM]
            ).astype(BF16)
            dk = scale * dot_nn(ds, qs_s[h])
            dk_s[:, h * NOPE : (h + 1) * NOPE] = dk[:, :NOPE].astype(BF16)
            rope_sum = rope_sum + dk[:, NOPE:]
            dqt_s[h] += dot_nn(kct_s[h], ds)
            if h == 0:

                @pl.when(n > first)
                def _():
                    stage_r2(n - 1)

            if h == heads // 2:

                @pl.when(n > first + 1)
                def _():
                    stage_r3(n - 2)

        @pl.when(n > first)
        def _():
            stage_b(n + 1)
            sends_done(n - 1)

        dlat = dot_nt(dk_s[...], wk_v[...]) + dot_nt(dv_s[...], wv_v[...])
        lat_all[j + 1, :, :latent_dim] = dlat.astype(BF16)
        lat_all[j + 1, :, latent_dim:] = rope_sum.astype(BF16)
        r1_copy(j).start()
        dvw_acc[...] += dot_nn(lat_all[j, :, :latent_dim].T, dv_s[...])

        @pl.when(n == first)
        def _():
            stage_a(jnp.int32(2))

            @pl.when(x == 0)
            def _():
                stage_a(jnp.int32(3))

        stage_a(n + 3)

        @pl.when(n == first)
        def _():
            stage_b(n + 1)

        return carry

    lax.fori_loop(first, last + 1, slot, 0)

    def dv_copy(d):
        k = (i + d) % ns
        return remote(
            dvw_b.at[k], dvw_rx.at[ns - d], dvs.at[d], dvr.at[ns - d], {"sp": k, "tp": t}
        )

    def dv_wait(d):
        k = (i + d) % ns
        return remote(dvw_b.at[k], dvw_rx.at[d], dvs.at[d], dvr.at[d], {"sp": k, "tp": t})

    for k in range(ns):
        dvw_b[k] = dvw_acc[k * lrows : (k + 1) * lrows, :].astype(BF16)
    for d in range(1, ns):
        dv_copy(d).start()

    stage_r2(last)

    @pl.when(last > first)
    def _():
        stage_r3(last - 1)

    for h in range(heads):
        dq_ref[:, h * width : (h + 1) * width] = (scale * dqt_s[h]).T[:, :width].astype(BF16)

    stage_r3(last)

    dvw = dvw_acc[pl.ds(pl.multiple_of(i * lrows, lrows), lrows), :]
    for d in range(1, ns):
        dv_wait(d).wait_recv()
        dvw = dvw + dvw_rx[d].astype(F32)
    dvw_ref[...] = dvw

    def add(k, carry):
        o_wait(k).wait_recv()
        own_acc[...] += orx[k].astype(F32)
        return carry

    lax.fori_loop(i + 1, ns, add, 0)
    fin[pl.ds(my_piece, piece), :] = own_acc[...].astype(BF16)

    def ag_y(d):
        yy = (y + d) % ny
        return remote(
            fin.at[pl.ds(my_piece, piece)], fin.at[pl.ds(my_piece, piece)], ags.at[d - 1], agr.at[d - 1],
            {"sp": i, "tp": yy * 2 + c},
        )

    def ag_y_wait(d):
        at = pl.multiple_of(c * half + ((y + ny - d) % ny) * piece, piece)
        return remote(
            fin.at[pl.ds(at, piece)], fin.at[pl.ds(at, piece)], ags.at[d - 1], agr.at[d - 1],
            {"sp": i, "tp": ((y + ny - d) % ny) * 2 + c},
        )

    for d in range(1, ny):
        ag_y(d).start()
    for d in range(1, ny):
        ag_y_wait(d).wait_recv()
    ag_c = remote(
        fin.at[pl.ds(my_half, half)], fin.at[pl.ds(my_half, half)], acs.at[0], acr.at[0], core_peer
    )
    ag_c_wait = remote(
        fin.at[pl.ds(peer_half, half)], fin.at[pl.ds(peer_half, half)], acs.at[0], acr.at[0], core_peer
    )
    ag_c.start()

    sends_done(last)

    def drain(n, carry):
        o_copy(block_of(n)).wait_send()
        return carry

    lax.fori_loop(first + 1, last + 1, drain, 0)
    for d in range(1, ns):
        dv_copy(d).wait_send()
    for d in range(1, ny):
        ag_y(d).wait_send()
    ag_c_wait.wait_recv()
    ag_c.wait_send()
    out = pltpu.make_async_copy(fin, dlat_hbm, ld.at[0])
    out.start()
    out.wait()


def fused_backward(ns, tp, queries, out_grad, attn_out, lse, latp, key_weight, value_weight):
    rows = queries.shape[0]
    latent_dim, hv = key_weight.shape
    heads = hv // NOPE
    packed = latp.shape[1]
    lrows = latent_dim // ns
    ny = tp // 2
    hbm = pl.BlockSpec(memory_space=pl.ANY)
    vmem = pl.BlockSpec(memory_space=pltpu.VMEM)
    dma = pltpu.SemaphoreType.DMA
    return pl.pallas_call(
        functools.partial(fused_kernel, ns, tp, heads, latent_dim),
        in_specs=[hbm, hbm, hbm, vmem, hbm, hbm, hbm],
        out_specs=[vmem, hbm, vmem],
        out_shape=[
            jax.ShapeDtypeStruct(queries.shape, BF16),
            jax.ShapeDtypeStruct((rows, packed), BF16),
            jax.ShapeDtypeStruct((lrows, hv), F32),
        ],
        scratch_shapes=[
            pltpu.VMEM(queries.shape, BF16),
            pltpu.VMEM(out_grad.shape, BF16),
            pltpu.VMEM(attn_out.shape, BF16),
            pltpu.VMEM(key_weight.shape, BF16),
            pltpu.VMEM(value_weight.shape, BF16),
            pltpu.VMEM((heads, rows, WIDE), BF16),
            pltpu.VMEM((heads, WIDE, rows), BF16),
            pltpu.VMEM((heads, VDIM, rows), BF16),
            pltpu.VMEM((heads, WIDE, rows), F32),
            pltpu.VMEM((heads, rows), F32),
            pltpu.VMEM((heads, rows, WIDE), BF16),
            pltpu.VMEM((heads, WIDE, rows), BF16),
            pltpu.VMEM((rows, hv), BF16),
            pltpu.VMEM((rows, hv), BF16),
            pltpu.VMEM((rows, hv), BF16),
            pltpu.VMEM((latent_dim, hv), F32),
            pltpu.VMEM((ns, lrows, hv), BF16),
            pltpu.VMEM((ns, lrows, hv), BF16),
            pltpu.VMEM((ns + 1, rows, packed), BF16),
            pltpu.VMEM((ns, rows // 2, packed), BF16),
            pltpu.VMEM((ns, max(ny - 1, 1), rows // tp, packed), BF16),
            pltpu.VMEM((ns, rows // tp, packed), BF16),
            pltpu.VMEM((rows // tp, packed), F32),
            pltpu.VMEM((rows, packed), BF16),
            dma((6,)),
            dma((ns,)),
            dma((ns,)),
            dma((1,)),
            dma((ns,)),
            dma((ns,)),
            dma((ns,)),
            dma((ns,)),
            dma((ns,)),
            dma((ns,)),
            dma((ns,)),
            dma((ns,)),
            dma((ns, max(ny - 1, 1))),
            dma((ns, max(ny - 1, 1))),
            dma((ns,)),
            dma((ns,)),
            dma((ns,)),
            dma((ns,)),
            dma((max(ny - 1, 1),)),
            dma((max(ny - 1, 1),)),
            dma((1,)),
            dma((1,)),
        ],
        compiler_params=pltpu.CompilerParams(
            collective_id=0, has_side_effects=True, vmem_limit_bytes=67043328
        ),
    )(queries, out_grad, attn_out, lse, latp, key_weight, value_weight)


def per_device(queries, latent, rope_key, key_weight, value_weight, log_sums, attn_out, out_grad):
    rows, latent_dim = latent.shape
    latp = jnp.concatenate(
        [latent, rope_key, jnp.zeros((rows, WIDE - NOPE - ROPE), BF16)], axis=1
    )
    d_queries, dlat, d_value_weight = fused_backward(
        lax.axis_size("sp"), lax.axis_size("tp"),
        queries, out_grad, attn_out, log_sums, latp, key_weight, value_weight,
    )
    d_latent = dlat[:, :latent_dim].astype(F32)
    d_rope = dlat[:, latent_dim : latent_dim + ROPE].astype(F32)
    return (d_queries, d_latent, d_rope, d_value_weight)


def solution(mesh):
    placed = (
        P("sp", "tp"),
        P("sp", None),
        P("sp", None),
        P(None, "tp"),
        P(None, "tp"),
        P("tp", "sp"),
        P("sp", "tp"),
        P("sp", "tp"),
    )
    return jax.shard_map(
        per_device,
        mesh=mesh,
        in_specs=placed,
        out_specs=(P("sp", "tp"), P("sp", None), P("sp", None), P("sp", "tp")),
        check_vma=False,
    )
```

time: 313 us -> 164 us (0.52)
  waiting for transfers between devices: 229 us -> 0 us
  Pallas kernels: 15.2 us -> 153 us
  starting transfers between devices: 41.8 us -> 0 us
  between operations: 13.8 us -> 0.66 us
  other arithmetic: 7.62 us -> 3.79 us
    pallas_call x1, Pallas kernels: 15.2 us -> 153 us  [fused_backward(): pl.pallas_call(functools.partial(fused_kernel, ns, tp, heads, latent_dim)...]
    reduce_scatter x1 -> x0, waiting for transfers between devices: 128 us -> none  [per_device(): lax.psum_scatter(dlat, ('sp', 'tp'), scatter_dimension=0, tiled=True)]
    all_gather x2 -> x0, waiting for transfers between devices: 100 us -> none  [the longest x1 83.3 us: per_device(): lat_all = lax.all_gather(piece, ('sp', 'tp'), axis=0, tiled=True)]
    all_to_all x1 -> x0, starting transfers between devices: 41.7 us -> none  [per_device(): dvw_parts = lax.all_to_all(dvw.astype(BF16), 'sp', 0, 0, tiled=True)]
  transfers between devices with their start and end apart: 4 -> 0, of which waited for: 3 -> 0; matrix products, arithmetic and copies ran while one was open for 2% -> 0% of each run, Pallas kernels for 0% -> 0%
where the time goes in v1:
time: 164 us
  Pallas kernels  153 us (93%)
  local copies, waits for them, and re-layouts  6.6 us (4%)
  other arithmetic  3.79 us (2%)
    pallas_call x1, Pallas kernels, fused_backward(): pl.pallas_call(functools.partial(fused_kernel, ns, tp, heads, latent_dim)...  153 us
    unnamed x8, local copies, waits for them, and re-layouts  3.53 us

profile of v1, /device:TPU:0, one launch (start us, length us, event | category | flops | bytes accessed | tf_op | source)
XLA Modules:
  0.0 163.7 jit_solution(7694677696262959208)
XLA Ops:
  0.6 1.0 copy.12
  1.6 3.1 %concatenate.3.latp_hbm = bf16[512,1152]{1,0:T(8,128)(2,1)} concatenate(bf16[512,1024]{1,0:T(8,128)(2,1)} %param.9, bf16[512,64]{1,0:T(8,128)(2,1)S(1)} %copy.12, bf16[512,64]{1,0:T(8,128)(2,1)S(1)} %broadcast_in_dim.3), dimensions={1} | concatenate | bytes 2359296 | tf_op jit(solution)/shard_map/concatenate | solution.py:557
  4.7 152.7 %shard_map.111 = (bf16[512,768]{1,0:T(8,128)(2,1)}, bf16[512,1152]{1,0:T(8,128)(2,1)}, f32[128,512]{1,0:T(8,128)}) custom-call(bf16[512,768]{1,0:T(8,128)(2,1)} %q_hbm.1, bf16[512,512]{1,0:T(8,128)(2,1)} %g_hbm.1, bf16[512,512]{1,0:T(8,128)(2,1)} %ao_hbm.1, f32[4,512]{1,0:T(4,128)} %lse_ref.1, bf16[512,1152]{1,0:T(8,128)(2,1)} %concatenate.3.latp_hbm, ...), custom_call_target="tpu_custom_call" | custom-call | tf_op jit(solution)/shard_map/pallas_call | solution.py:492
  157.4 0.9 slice_convert_fusion.1
  158.3 0.8 copy.13
  159.1 0.0 copy-start
  159.1 2.9 %slice_convert_fusion = f32[512,1024]{1,0:T(8,128)} fusion(bf16[512,1152]{1,0:T(8,128)(2,1)} %get-tuple-element.8), kind=kLoop, calls=%fused_computation | loop fusion | flops 524288 | bytes 3145728 | tf_op jit(solution)/shard_map/convert_element_type | solution.py:564
  161.9 0.0 copy-done
  161.9 0.0 copy-start.1
  161.9 0.9 copy.16
  162.8 0.2 copy-done.1
  163.0 0.7 copy.17
  (1 shorter events, 0.0 us)
Async XLA Ops:
  159.1 2.9 %copy-start = (bf16[512,768]{1,0:T(8,128)(2,1)S(1)}, bf16[512,768]{1,0:T(8,128)(2,1)}, u32[]{:S(2)}) copy-start(bf16[512,768]{1,0:T(8,128)(2,1)} %get-tuple-element.18) | copy-start | bytes 2359300
  161.9 1.1 copy-start.1

commit v2 on v1

v2 whole, which is shorter than its diff:
```python
import functools

import jax
import jax.numpy as jnp
from jax import lax
from jax.experimental import pallas as pl
from jax.experimental.pallas import tpu as pltpu
from jax.sharding import PartitionSpec as P

NOPE = 128
ROPE = 64
VDIM = 128
WIDE = 256
LOG2E = 1.4426950408889634
BF16 = jnp.bfloat16
F32 = jnp.float32
MESH = pl.DeviceIdType.MESH


def dot_nn(a, b):
    return lax.dot_general(a, b, (((1,), (0,)), ((), ())), preferred_element_type=F32)


def dot_nt(a, b):
    return lax.dot_general(a, b, (((1,), (1,)), ((), ())), preferred_element_type=F32)


def fused_kernel(
    ns,
    tp,
    heads,
    latent_dim,
    q_hbm,
    g_hbm,
    ao_hbm,
    lse_ref,
    lat_hbm,
    rope_hbm,
    wk_hbm,
    wv_hbm,
    dq_ref,
    dlat_hbm,
    drope_hbm,
    dvw_ref,
    q_v,
    g_v,
    ao_v,
    wk_v,
    wv_v,
    qs_s,
    qt_s,
    gt_s,
    dqt_s,
    delta_s,
    kc_s,
    kct_s,
    v_s,
    dk_s,
    dv_s,
    dvw_acc,
    dvw_b,
    dvw_rx,
    lat_all,
    crx,
    yrx,
    xrx,
    orx,
    own_acc,
    fin,
    ld,
    zr,
    zs,
    xr,
    xs,
    cr,
    cs,
    xrr,
    xrs,
    r1r,
    r1s,
    yr,
    ys,
    orr,
    ors,
    dvr,
    dvs,
    agr,
    ags,
    acr,
    acs,
):
    i = lax.axis_index("sp")
    t = lax.axis_index("tp")
    ny = tp // 2
    nz = ns // 2
    z, x = i // 2, i % 2
    y, c = t // 2, t % 2
    rows, width = q_v.shape[0], NOPE + ROPE
    half, quart, piece = rows // 2, rows // 4, rows // tp
    scale = width ** (-0.5)
    lrows = latent_dim // ns

    lower = 2 * z
    last = lower + x

    def block_of(n):
        down = 2 * (z - 1 - (n - 1) // 2) + (x + n - 1) % 2
        return lax.select(n == 0, i, lax.select(n > lower, jnp.int32(2 * z), down))

    def part_of(n):
        return lax.select(n == 0, jnp.int32(ns), lax.select(n == 1, jnp.int32(ns + 1), block_of(n - 1)))

    def own_column(n):
        return jnp.logical_and(n % 2 == 1, n <= lower)

    def other_column(n):
        return jnp.logical_and(n >= 1, jnp.logical_or(n % 2 == 0, n > lower))

    my_half = pl.multiple_of(c * half, half)
    peer_half = pl.multiple_of((1 - c) * half, half)
    core_peer = {"sp": i, "tp": y * 2 + 1 - c}
    x_peer = {"sp": 2 * z + 1 - x, "tp": t}
    above = {"sp": lax.min(i + 2, ns - 1), "tp": t}

    def remote(src, dst, ssem, rsem, dev):
        return pltpu.make_async_remote_copy(
            src_ref=src, dst_ref=dst, send_sem=ssem, recv_sem=rsem, device_id=dev, device_id_type=MESH
        )

    def lat_rows(j, at, size):
        return lat_all.at[j, pl.ds(at, size)]

    own_cps = [
        pltpu.make_async_copy(lat_hbm, lat_all.at[i, :, pl.ds(0, latent_dim)], ld.at[0]),
        pltpu.make_async_copy(rope_hbm, lat_all.at[i, :, pl.ds(latent_dim, WIDE - NOPE)], ld.at[6]),
    ]
    loads = [
        pltpu.make_async_copy(s, d, ld.at[k + 1])
        for k, (s, d) in enumerate(
            ((g_hbm, g_v), (q_hbm, q_v), (ao_hbm, ao_v), (wk_hbm, wk_v), (wv_hbm, wv_v))
        )
    ]
    for cp in own_cps + loads:
        cp.start()

    barrier = pltpu.get_barrier_semaphore()
    for d in range(1, ns):
        pl.semaphore_signal(
            barrier, inc=1, device_id={"sp": (i + d) % ns, "tp": t}, device_id_type=MESH
        )
    for d in range(1, tp):
        pl.semaphore_signal(
            barrier, inc=1, device_id={"sp": i, "tp": (t + d) % tp}, device_id_type=MESH
        )
    pl.semaphore_wait(barrier, ns - 1 + tp - 1)
    for cp in own_cps:
        cp.wait()

    def quarter(j, k):
        return lat_rows(j, pl.multiple_of(c * half + k * quart, quart), quart)

    def z_copy(j, k):
        return remote(quarter(j, k), quarter(j, k), zs.at[j, k], zr.at[j, k], above)

    def x_copy(j, k):
        return remote(quarter(j, k), quarter(j, k), xs.at[j, k], xr.at[j, k], x_peer)

    def c_copy(j):
        return remote(lat_rows(j, my_half, half), lat_rows(j, my_half, half), cs.at[j], cr.at[j], core_peer)

    has_next = z + 1 < nz

    @pl.when(has_next)
    def _():
        z_copy(i, 0).start()
        z_copy(i, 1).start()

    @pl.when(x == 0)
    def _():
        x_copy(i, 0).start()

    def stage_a(n, k):
        @pl.when(own_column(n))
        def _():
            j = block_of(n)
            z_copy(j, k).wait_recv()
            x_copy(j, k).start()

            @pl.when(has_next)
            def _():
                z_copy(j, k).start()

            if k == 1:
                c_copy(j).start()

    def stage_b(n):
        @pl.when(jnp.logical_and(other_column(n), n <= last))
        def _():
            j = block_of(n)
            x_copy(j, 0).wait_recv()
            x_copy(j, 1).wait_recv()
            c_copy(j).start()

    def sends_done(n):
        j = block_of(n)
        c_copy(j).wait_send()

        @pl.when(own_column(n))
        def _():
            for k in range(2):
                x_copy(j, k).wait_send()

            @pl.when(has_next)
            def _():
                for k in range(2):
                    z_copy(j, k).wait_send()

    def r1_copy(n):
        j = block_of(n)
        return remote(
            lat_rows(part_of(n), peer_half, half), crx.at[j], r1s.at[j], r1r.at[j], core_peer
        )

    def y_copy(n, d):
        j = block_of(n)
        yy = (y + d) % ny
        at = pl.multiple_of(c * half + yy * piece, piece)
        return remote(
            lat_rows(part_of(n), at, piece), yrx.at[j, d - 1], ys.at[j, d - 1], yr.at[j, d - 1],
            {"sp": i, "tp": yy * 2 + c},
        )

    my_piece = pl.multiple_of(c * half + y * piece, piece)

    def xr_copy(n):
        j = block_of(n)
        return remote(lat_rows(part_of(n), my_piece, piece), xrx.at[j], xrs.at[j], xrr.at[j], x_peer)

    def o_copy(n):
        j = block_of(n)
        return remote(
            lat_rows(part_of(n), my_piece, piece), orx.at[z], ors.at[j], orr.at[z], {"sp": j, "tp": t}
        )

    def o_wait(zz):
        return remote(
            lat_rows(i, my_piece, piece), orx.at[zz], ors.at[i], orr.at[zz], x_peer
        )

    def stage_r2(n):
        j = block_of(n)
        b = part_of(n)
        r1_copy(n).wait_recv()
        mine = lat_all[b, pl.ds(my_half, half), :].astype(F32)
        lat_all[b, pl.ds(my_half, half), :] = (mine + crx[j].astype(F32)).astype(BF16)
        for d in range(1, ny):
            y_copy(n, d).start()

    def stage_r3(n):
        j = block_of(n)
        b = part_of(n)
        total = lat_all[b, pl.ds(my_piece, piece), :].astype(F32)
        for d in range(1, ny):
            y_copy(n, d).wait_recv()
            total = total + yrx[j, d - 1].astype(F32)
        for d in range(1, ny):
            y_copy(n, d).wait_send()
        r1_copy(n).wait_send()

        @pl.when(n == 0)
        def _():
            own_acc[...] = total

        @pl.when(n > 0)
        def _():
            lat_all[b, pl.ds(my_piece, piece), :] = total.astype(BF16)

        @pl.when(jnp.logical_and(other_column(n), n <= lower))
        def _():
            xr_copy(n).start()

        @pl.when(n > lower)
        def _():
            @pl.when(n > 0)
            def _():
                o_copy(n).start()

    def stage_r4(n):
        @pl.when(own_column(n))
        def _():
            j = block_of(n)
            b = part_of(n)
            xr_copy(n).wait_recv()
            total = lat_all[b, pl.ds(my_piece, piece), :].astype(F32) + xrx[j].astype(F32)
            lat_all[b, pl.ds(my_piece, piece), :] = total.astype(BF16)
            o_copy(n).start()

    for cp in loads:
        cp.wait()
    for h in range(heads):
        qh = jnp.concatenate(
            [q_v[:, h * width : (h + 1) * width], jnp.zeros((rows, WIDE - width), BF16)], axis=1
        )
        qs_s[h] = qh
        qt_s[h] = qh.T
        gt = g_v[:, h * VDIM : (h + 1) * VDIM].T
        gt_s[h] = gt
        at = ao_v[:, h * VDIM : (h + 1) * VDIM].T
        delta_s[h : h + 1, :] = jnp.sum(gt.astype(F32) * at.astype(F32), axis=0, keepdims=True)
    dqt_s[...] = jnp.zeros_like(dqt_s)
    dvw_acc[...] = jnp.zeros_like(dvw_acc)

    def slot(n, carry):
        j = block_of(n)
        b = part_of(n)

        @pl.when(n > 0)
        def _():
            c_copy(j).wait_recv()

        rope = lat_all[j, :, latent_dim:]
        keys = dot_nn(lat_all[j, :, :latent_dim], wk_v[...]).astype(BF16)
        v_s[...] = dot_nn(lat_all[j, :, :latent_dim], wv_v[...]).astype(BF16)
        for h in range(heads):
            kc = jnp.concatenate([keys[:, h * NOPE : (h + 1) * NOPE], rope], axis=1)
            kc_s[h] = kc
            kct_s[h] = kc.T
        rope_sum = jnp.zeros((rows, WIDE - NOPE), F32)
        k_pos = lax.broadcasted_iota(jnp.int32, (rows, rows), 0)
        q_pos = lax.broadcasted_iota(jnp.int32, (rows, rows), 1)
        causal = k_pos - q_pos <= (i - j) * rows
        for h in range(heads):
            s = dot_nn(kc_s[h], qt_s[h])
            zz = s * (scale * LOG2E) - lse_ref[h : h + 1, :] * LOG2E
            p = jnp.exp2(jnp.where(causal, zz, -1e30))
            dp = dot_nn(v_s[:, h * VDIM : (h + 1) * VDIM], gt_s[h])
            ds = (p * (dp - delta_s[h : h + 1, :])).astype(BF16)
            dv_s[:, h * VDIM : (h + 1) * VDIM] = dot_nn(
                p.astype(BF16), g_v[:, h * VDIM : (h + 1) * VDIM]
            ).astype(BF16)
            dk = scale * dot_nn(ds, qs_s[h])
            dk_s[:, h * NOPE : (h + 1) * NOPE] = dk[:, :NOPE].astype(BF16)
            rope_sum = rope_sum + dk[:, NOPE:]
            dqt_s[h] += dot_nn(kct_s[h], ds)
            if h == 0:

                @pl.when(n > 0)
                def _():
                    stage_r2(n - 1)

            if h == (heads - 1) // 2:

                @pl.when(n > 1)
                def _():
                    stage_a(n + 1, 1)

            if h == heads // 2:

                @pl.when(n > 1)
                def _():
                    stage_r3(n - 2)

                @pl.when(n == 0)
                def _():
                    stage_a(n + 1, 0)

        @pl.when(n > 4)
        def _():
            stage_r4(n - 4)

        @pl.when(n > 1)
        def _():
            sends_done(n - 1)

        dlat = dot_nt(dk_s[...], wk_v[...]) + dot_nt(dv_s[...], wv_v[...])
        lat_all[b, :, :latent_dim] = dlat.astype(BF16)
        lat_all[b, :, latent_dim:] = rope_sum.astype(BF16)
        r1_copy(n).start()

        @pl.when(n == 0)
        def _():
            stage_a(n + 1, 1)

        stage_b(n + 1)
        dvw_acc[...] += dot_nn(lat_all[j, :, :latent_dim].T, dv_s[...])

        @pl.when(n > 0)
        def _():
            stage_a(n + 2, 0)

        @pl.when(jnp.logical_and(x == 0, n == lax.min(2, last)))
        def _():
            x_copy(i, 1).start()

        return carry

    lax.fori_loop(0, last + 1, slot, 0)

    def dv_copy(d):
        k = (i + d) % ns
        return remote(
            dvw_b.at[k], dvw_rx.at[ns - d], dvs.at[d], dvr.at[ns - d], {"sp": k, "tp": t}
        )

    def dv_wait(d):
        k = (i + d) % ns
        return remote(dvw_b.at[k], dvw_rx.at[d], dvs.at[d], dvr.at[d], {"sp": k, "tp": t})

    for k in range(ns):
        dvw_b[k] = dvw_acc[k * lrows : (k + 1) * lrows, :].astype(BF16)
    for d in range(1, ns):
        dv_copy(d).start()

    stage_r2(last)

    @pl.when(last > 3)
    def _():
        stage_r4(last - 3)

    @pl.when(last > 0)
    def _():
        stage_r3(last - 1)

    for h in range(heads):
        dq_ref[:, h * width : (h + 1) * width] = (scale * dqt_s[h]).T[:, :width].astype(BF16)

    stage_r3(last)

    def tail(n, carry):
        stage_r4(n)
        return carry

    lax.fori_loop(lax.max(last - 2, 1), lower + 1, tail, 0)

    dvw = dvw_acc[pl.ds(pl.multiple_of(i * lrows, lrows), lrows), :]
    for d in range(1, ns):
        dv_wait(d).wait_recv()
        dvw = dvw + dvw_rx[d].astype(F32)
    dvw_ref[...] = dvw

    def add(k, carry):
        o_wait(k).wait_recv()
        own_acc[...] += orx[k].astype(F32)
        return carry

    @pl.when(x == 0)
    def _():
        add(z, 0)

    lax.fori_loop(z + 1, nz, add, 0)
    fin[pl.ds(my_piece, piece), :] = own_acc[...].astype(BF16)

    def ag_y(d):
        yy = (y + d) % ny
        return remote(
            fin.at[pl.ds(my_piece, piece)], fin.at[pl.ds(my_piece, piece)], ags.at[d - 1], agr.at[d - 1],
            {"sp": i, "tp": yy * 2 + c},
        )

    def ag_y_wait(d):
        at = pl.multiple_of(c * half + ((y + ny - d) % ny) * piece, piece)
        return remote(
            fin.at[pl.ds(at, piece)], fin.at[pl.ds(at, piece)], ags.at[d - 1], agr.at[d - 1],
            {"sp": i, "tp": ((y + ny - d) % ny) * 2 + c},
        )

    for d in range(1, ny):
        ag_y(d).start()
    for d in range(1, ny):
        ag_y_wait(d).wait_recv()
    ag_c = remote(
        fin.at[pl.ds(my_half, half)], fin.at[pl.ds(my_half, half)], acs.at[0], acr.at[0], core_peer
    )
    ag_c_wait = remote(
        fin.at[pl.ds(peer_half, half)], fin.at[pl.ds(peer_half, half)], acs.at[0], acr.at[0], core_peer
    )
    ag_c.start()

    @pl.when(last > 0)
    def _():
        sends_done(last)

    @pl.when(has_next)
    def _():
        z_copy(i, 0).wait_send()
        z_copy(i, 1).wait_send()

    @pl.when(x == 0)
    def _():
        x_copy(i, 0).wait_send()
        x_copy(i, 1).wait_send()

    def drain(n, carry):
        @pl.when(jnp.logical_or(own_column(n), n > lower))
        def _():
            o_copy(n).wait_send()

        @pl.when(jnp.logical_and(other_column(n), n <= lower))
        def _():
            xr_copy(n).wait_send()

        return carry

    lax.fori_loop(1, last + 1, drain, 0)
    for d in range(1, ns):
        dv_copy(d).wait_send()
    for d in range(1, ny):
        ag_y(d).wait_send()
    ag_c_wait.wait_recv()
    ag_c.wait_send()
    outs = [
        pltpu.make_async_copy(fin.at[:, pl.ds(0, latent_dim)], dlat_hbm, ld.at[0]),
        pltpu.make_async_copy(fin.at[:, pl.ds(latent_dim, WIDE - NOPE)], drope_hbm, ld.at[6]),
    ]
    for out in outs:
        out.start()
    for out in outs:
        out.wait()


def fused_backward(ns, tp, queries, out_grad, attn_out, lse, latent, rope, key_weight, value_weight):
    rows = queries.shape[0]
    latent_dim, hv = key_weight.shape
    heads = hv // NOPE
    packed = latent_dim + rope.shape[1]
    lrows = latent_dim // ns
    ny = tp // 2
    hbm = pl.BlockSpec(memory_space=pl.ANY)
    vmem = pl.BlockSpec(memory_space=pltpu.VMEM)
    dma = pltpu.SemaphoreType.DMA
    return pl.pallas_call(
        functools.partial(fused_kernel, ns, tp, heads, latent_dim),
        in_specs=[hbm, hbm, hbm, vmem, hbm, hbm, hbm, hbm],
        out_specs=[vmem, hbm, hbm, vmem],
        out_shape=[
            jax.ShapeDtypeStruct(queries.shape, BF16),
            jax.ShapeDtypeStruct(latent.shape, BF16),
            jax.ShapeDtypeStruct(rope.shape, BF16),
            jax.ShapeDtypeStruct((lrows, hv), F32),
        ],
        scratch_shapes=[
            pltpu.VMEM(queries.shape, BF16),
            pltpu.VMEM(out_grad.shape, BF16),
            pltpu.VMEM(attn_out.shape, BF16),
            pltpu.VMEM(key_weight.shape, BF16),
            pltpu.VMEM(value_weight.shape, BF16),
            pltpu.VMEM((heads, rows, WIDE), BF16),
            pltpu.VMEM((heads, WIDE, rows), BF16),
            pltpu.VMEM((heads, VDIM, rows), BF16),
            pltpu.VMEM((heads, WIDE, rows), F32),
            pltpu.VMEM((heads, rows), F32),
            pltpu.VMEM((heads, rows, WIDE), BF16),
            pltpu.VMEM((heads, WIDE, rows), BF16),
            pltpu.VMEM((rows, hv), BF16),
            pltpu.VMEM((rows, hv), BF16),
            pltpu.VMEM((rows, hv), BF16),
            pltpu.VMEM((latent_dim, hv), F32),
            pltpu.VMEM((ns, lrows, hv), BF16),
            pltpu.VMEM((ns, lrows, hv), BF16),
            pltpu.VMEM((ns + 2, rows, packed), BF16),
            pltpu.VMEM((ns, rows // 2, packed), BF16),
            pltpu.VMEM((ns, max(ny - 1, 1), rows // tp, packed), BF16),
            pltpu.VMEM((ns, rows // tp, packed), BF16),
            pltpu.VMEM((ns // 2, rows // tp, packed), BF16),
            pltpu.VMEM((rows // tp, packed), F32),
            pltpu.VMEM((rows, packed), BF16),
            dma((7,)),
            dma((ns, 2)),
            dma((ns, 2)),
            dma((ns, 2)),
            dma((ns, 2)),
            dma((ns,)),
            dma((ns,)),
            dma((ns,)),
            dma((ns,)),
            dma((ns,)),
            dma((ns,)),
            dma((ns, max(ny - 1, 1))),
            dma((ns, max(ny - 1, 1))),
            dma((ns // 2,)),
            dma((ns,)),
            dma((ns,)),
            dma((ns,)),
            dma((max(ny - 1, 1),)),
            dma((max(ny - 1, 1),)),
            dma((1,)),
            dma((1,)),
        ],
        compiler_params=pltpu.CompilerParams(
            collective_id=0, has_side_effects=True, vmem_limit_bytes=67043328
        ),
    )(queries, out_grad, attn_out, lse, latent, rope, key_weight, value_weight)


def per_device(queries, latent, rope_key, key_weight, value_weight, log_sums, attn_out, out_grad):
    rope = jnp.pad(rope_key, ((0, 0), (0, WIDE - NOPE - ROPE)))
    d_queries, dlat, drope, d_value_weight = fused_backward(
        lax.axis_size("sp"), lax.axis_size("tp"),
        queries, out_grad, attn_out, log_sums, latent, rope, key_weight, value_weight,
    )
    d_latent = dlat.astype(F32)
    d_rope = drope[:, :ROPE].astype(F32)
    return (d_queries, d_latent, d_rope, d_value_weight)


def solution(mesh):
    placed = (
        P("sp", "tp"),
        P("sp", None),
        P("sp", None),
        P(None, "tp"),
        P(None, "tp"),
        P("tp", "sp"),
        P("sp", "tp"),
        P("sp", "tp"),
    )
    return jax.shard_map(
        per_device,
        mesh=mesh,
        in_specs=placed,
        out_specs=(P("sp", "tp"), P("sp", None), P("sp", None), P("sp", "tp")),
        check_vma=False,
    )
```

time: 164 us -> 149 us (0.909)
  the two profiles are of different devices: /device:TPU:0 before, /device:TPU:3 now
where the time goes in v2:
time: 149 us
  Pallas kernels  140 us (94%)
  local copies, waits for them, and re-layouts  4.01 us (3%)
  other arithmetic  3.83 us (3%)
    pallas_call x1, Pallas kernels, fused_backward(): pl.pallas_call(functools.partial(fused_kernel, ns, tp, heads, latent_dim)...  140 us
    unnamed x8, local copies, waits for them, and re-layouts  3.32 us

profile of v2, /device:TPU:3, one launch (start us, length us, event | category | flops | bytes accessed | tf_op | source)
XLA Modules:
  0.0 148.8 jit_solution(608788248956274364)
XLA Ops:
  0.6 1.0 copy.12
  1.6 0.7 pad.4.rope_hbm
  2.3 140.3 %shard_map.111 = (bf16[512,768]{1,0:T(8,128)(2,1)}, bf16[512,1024]{1,0:T(8,128)(2,1)}, bf16[512,128]{1,0:T(8,128)(2,1)}, f32[128,512]{1,0:T(8,128)}) custom-call(bf16[512,768]{1,0:T(8,128)(2,1)} %q_hbm.1, bf16[512,512]{1,0:T(8,128)(2,1)} %g_hbm.1, bf16[512,512]{1,0:T(8,128)(2,1)} %ao_hbm.1, f32[4,512]{1,0:T(4,128)} %lse_ref.1, bf16[512,1024]{1,0:T(8,128)(2,1)} %lat_hbm.1, ...), custom_call_target="tpu_custom_call" | custom-call | tf_op jit(solution)/shard_map/pallas_call | solution.py:531
  142.6 0.0 copy-start
  142.6 1.0 slice_convert_fusion
  143.6 0.8 copy.13
  144.3 0.0 copy-start.1
  144.3 2.8 %convert_element_type.8 = f32[512,1024]{1,0:T(8,128)} convert(bf16[512,1024]{1,0:T(8,128)(2,1)} %get-tuple-element.9) | non-fusion elementwise | flops 524288 | bytes 3145728 | tf_op jit(solution)/shard_map/convert_element_type | solution.py:601
  147.2 0.0 copy-done
  147.2 0.9 copy.16
  148.1 0.0 copy-done.1
  148.1 0.7 copy.17
Async XLA Ops:
  142.6 4.6 %copy-start = (bf16[512,768]{1,0:T(8,128)(2,1)S(1)}, bf16[512,768]{1,0:T(8,128)(2,1)}, u32[]{:S(2)}) copy-start(bf16[512,768]{1,0:T(8,128)(2,1)} %get-tuple-element.20) | copy-start | bytes 2359300
  144.3 3.7 %copy-start.1 = (f32[128,512]{1,0:T(8,128)S(1)}, f32[128,512]{1,0:T(8,128)}, u32[]{:S(2)}) copy-start(f32[128,512]{1,0:T(8,128)} %get-tuple-element.23) | copy-start | bytes 786436

commit v3 on v2

--- a/solution.py
+++ b/solution.py
@@ -44,6 +44,8 @@
     dvw_ref,
     q_v,
     g_v,
+    fq_v,
+    lse_s,
     ao_v,
     wk_v,
     wv_v,
@@ -88,6 +90,8 @@
     ags,
     acr,
     acs,
+    vr,
+    vs,
 ):
     i = lax.axis_index("sp")
     t = lax.axis_index("tp")
@@ -100,21 +104,42 @@
     scale = width ** (-0.5)
     lrows = latent_dim // ns
 
-    lower = 2 * z
-    last = lower + x
+    top = nz - 1
+    is_top, is_low = z == top, z == 0
+    lower = lax.select(is_top, 2 * (z - 1), 2 * z)
+    base = lower + x
+    last = base + lax.select(is_low, jnp.int32(2), jnp.int32(0))
+
+    def visiting(n):
+        return n > base
 
     def block_of(n):
         down = 2 * (z - 1 - (n - 1) // 2) + (x + n - 1) % 2
-        return lax.select(n == 0, i, lax.select(n > lower, jnp.int32(2 * z), down))
+        home = lax.select(n == 0, i, lax.select(n > lower, jnp.int32(2 * z), down))
+        return lax.select(visiting(n), lax.select(n == base + 1, i, 1 - i), home)
+
+    def key_of(n):
+        return lax.select(visiting(n), block_of(n) + 2, block_of(n))
 
     def part_of(n):
-        return lax.select(n == 0, jnp.int32(ns), lax.select(n == 1, jnp.int32(ns + 1), block_of(n - 1)))
+        later = lax.select(is_low, n, block_of(n - 1))
+        return lax.select(n == 0, jnp.int32(ns), lax.select(n == 1, jnp.int32(ns + 1), later))
 
     def own_column(n):
         return jnp.logical_and(n % 2 == 1, n <= lower)
 
-    def other_column(n):
-        return jnp.logical_and(n >= 1, jnp.logical_or(n % 2 == 0, n > lower))
+    def for_x_sum(n):
+        return jnp.logical_and(jnp.logical_and(n >= 1, n <= lower), n % 2 == 0)
+
+    def in_plane(n):
+        return jnp.logical_and(x == 1, n == lower + 1)
+
+    def by_x(n):
+        mine = jnp.logical_and(is_low, jnp.logical_and(x == 0, n == base + 2))
+        return jnp.logical_or(for_x_sum(n), jnp.logical_or(in_plane(n), mine))
+
+    def visit_out(n):
+        return jnp.logical_and(is_low, n == base + 2)
 
     my_half = pl.multiple_of(c * half, half)
     peer_half = pl.multiple_of((1 - c) * half, half)
@@ -137,7 +162,7 @@
     loads = [
         pltpu.make_async_copy(s, d, ld.at[k + 1])
         for k, (s, d) in enumerate(
-            ((g_hbm, g_v), (q_hbm, q_v), (ao_hbm, ao_v), (wk_hbm, wk_v), (wv_hbm, wv_v))
+            ((g_hbm, g_v.at[0]), (q_hbm, q_v), (ao_hbm, ao_v), (wk_hbm, wk_v), (wv_hbm, wv_v))
         )
     ]
     for cp in own_cps + loads:
@@ -175,9 +200,27 @@
         z_copy(i, 0).start()
         z_copy(i, 1).start()
 
-    @pl.when(x == 0)
+    @pl.when(jnp.logical_or(x == 0, is_low))
     def _():
         x_copy(i, 0).start()
+
+    @pl.when(is_low)
+    def _():
+        x_copy(i, 1).start()
+
+    def goes_on(n):
+        return jnp.logical_and(has_next, jnp.logical_or(z + 1 != top, block_of(n) >= 2))
+
+    low_peer = {"sp": x, "tp": t}
+    top_peer = {"sp": 2 * top + x, "tp": t}
+
+    visits = ((g_v.at[0], g_v.at[1]), (q_v, fq_v), (lse_ref, lse_s.at[1]), (delta_s.at[0], delta_s.at[1]))
+
+    def visit_copy(k):
+        return remote(visits[k][0], visits[k][1], vs.at[k], vr.at[k], low_peer)
+
+    def back_copy():
+        return remote(fq_v, fq_v, vs.at[4], vr.at[4], top_peer)
 
     def stage_a(n, k):
         @pl.when(own_column(n))
@@ -186,7 +229,7 @@
             z_copy(j, k).wait_recv()
             x_copy(j, k).start()
 
-            @pl.when(has_next)
+            @pl.when(goes_on(n))
             def _():
                 z_copy(j, k).start()
 
@@ -194,7 +237,7 @@
                 c_copy(j).start()
 
     def stage_b(n):
-        @pl.when(jnp.logical_and(other_column(n), n <= last))
+        @pl.when(by_x(n))
         def _():
             j = block_of(n)
             x_copy(j, 0).wait_recv()
@@ -203,26 +246,29 @@
 
     def sends_done(n):
         j = block_of(n)
-        c_copy(j).wait_send()
+
+        @pl.when(jnp.logical_or(own_column(n), by_x(n)))
+        def _():
+            c_copy(j).wait_send()
 
         @pl.when(own_column(n))
         def _():
             for k in range(2):
                 x_copy(j, k).wait_send()
 
-            @pl.when(has_next)
+            @pl.when(goes_on(n))
             def _():
                 for k in range(2):
                     z_copy(j, k).wait_send()
 
     def r1_copy(n):
-        j = block_of(n)
+        j = key_of(n)
         return remote(
             lat_rows(part_of(n), peer_half, half), crx.at[j], r1s.at[j], r1r.at[j], core_peer
         )
 
     def y_copy(n, d):
-        j = block_of(n)
+        j = key_of(n)
         yy = (y + d) % ny
         at = pl.multiple_of(c * half + yy * piece, piece)
         return remote(
@@ -237,9 +283,14 @@
         return remote(lat_rows(part_of(n), my_piece, piece), xrx.at[j], xrs.at[j], xrr.at[j], x_peer)
 
     def o_copy(n):
-        j = block_of(n)
         return remote(
-            lat_rows(part_of(n), my_piece, piece), orx.at[z], ors.at[j], orr.at[z], {"sp": j, "tp": t}
+            lat_rows(part_of(n), my_piece, piece), orx.at[z], ors.at[key_of(n)], orr.at[z],
+            {"sp": block_of(n), "tp": t},
+        )
+
+    def v_copy(n):
+        return remote(
+            lat_rows(part_of(n), my_piece, piece), orx.at[nz], ors.at[key_of(n)], orr.at[nz], x_peer
         )
 
     def o_wait(zz):
@@ -248,7 +299,7 @@
         )
 
     def stage_r2(n):
-        j = block_of(n)
+        j = key_of(n)
         b = part_of(n)
         r1_copy(n).wait_recv()
         mine = lat_all[b, pl.ds(my_half, half), :].astype(F32)
@@ -257,7 +308,7 @@
             y_copy(n, d).start()
 
     def stage_r3(n):
-        j = block_of(n)
+        j = key_of(n)
         b = part_of(n)
         total = lat_all[b, pl.ds(my_piece, piece), :].astype(F32)
         for d in range(1, ny):
@@ -271,19 +322,25 @@
         def _():
             own_acc[...] = total
 
+        @pl.when(jnp.logical_and(is_low, n == base + 1))
+        def _():
+            own_acc[...] += total
+
         @pl.when(n > 0)
         def _():
             lat_all[b, pl.ds(my_piece, piece), :] = total.astype(BF16)
 
-        @pl.when(jnp.logical_and(other_column(n), n <= lower))
+        @pl.when(for_x_sum(n))
         def _():
             xr_copy(n).start()
 
-        @pl.when(n > lower)
-        def _():
-            @pl.when(n > 0)
-            def _():
-                o_copy(n).start()
+        @pl.when(in_plane(n))
+        def _():
+            o_copy(n).start()
+
+        @pl.when(visit_out(n))
+        def _():
+            v_copy(n).start()
 
     def stage_r4(n):
         @pl.when(own_column(n))
@@ -295,28 +352,55 @@
             lat_all[b, pl.ds(my_piece, piece), :] = total.astype(BF16)
             o_copy(n).start()
 
-    for cp in loads:
+    def prepare(qi, q_ref):
+        for h in range(heads):
+            qh = jnp.concatenate(
+                [q_ref[:, h * width : (h + 1) * width], jnp.zeros((rows, WIDE - width), BF16)], axis=1
+            )
+            qs_s[qi, h] = qh
+            qt_s[qi, h] = qh.T
+            gt_s[qi, h] = g_v[qi, :, h * VDIM : (h + 1) * VDIM].T
+        dqt_s[qi] = jnp.zeros_like(dqt_s[qi])
+
+    for cp in loads[:2]:
         cp.wait()
+
+    @pl.when(is_top)
+    def _():
+        for k in range(3):
+            visit_copy(k).start()
+
+    for cp in loads[2:]:
+        cp.wait()
+    prepare(0, q_v)
     for h in range(heads):
-        qh = jnp.concatenate(
-            [q_v[:, h * width : (h + 1) * width], jnp.zeros((rows, WIDE - width), BF16)], axis=1
-        )
-        qs_s[h] = qh
-        qt_s[h] = qh.T
-        gt = g_v[:, h * VDIM : (h + 1) * VDIM].T
-        gt_s[h] = gt
         at = ao_v[:, h * VDIM : (h + 1) * VDIM].T
-        delta_s[h : h + 1, :] = jnp.sum(gt.astype(F32) * at.astype(F32), axis=0, keepdims=True)
-    dqt_s[...] = jnp.zeros_like(dqt_s)
+        delta_s[0, h : h + 1, :] = jnp.sum(
+            gt_s[0, h].astype(F32) * at.astype(F32), axis=0, keepdims=True
+        )
+    lse_s[0] = lse_ref[...]
+
+    @pl.when(is_top)
+    def _():
+        visit_copy(3).start()
+
     dvw_acc[...] = jnp.zeros_like(dvw_acc)
 
     def slot(n, carry):
         j = block_of(n)
         b = part_of(n)
-
-        @pl.when(n > 0)
+        qi = lax.select(visiting(n), jnp.int32(1), jnp.int32(0))
+        q_block = lax.select(visiting(n), 2 * top + x, i)
+
+        @pl.when(jnp.logical_or(own_column(n), by_x(n)))
         def _():
             c_copy(j).wait_recv()
+
+        @pl.when(n == base + 1)
+        def _():
+            for k in range(4):
+                visit_copy(k).wait_recv()
+            prepare(1, fq_v)
 
         rope = lat_all[j, :, latent_dim:]
         keys = dot_nn(lat_all[j, :, :latent_dim], wk_v[...]).astype(BF16)
@@ -328,20 +412,20 @@
         rope_sum = jnp.zeros((rows, WIDE - NOPE), F32)
         k_pos = lax.broadcasted_iota(jnp.int32, (rows, rows), 0)
         q_pos = lax.broadcasted_iota(jnp.int32, (rows, rows), 1)
-        causal = k_pos - q_pos <= (i - j) * rows
+        causal = k_pos - q_pos <= (q_block - j) * rows
         for h in range(heads):
-            s = dot_nn(kc_s[h], qt_s[h])
-            zz = s * (scale * LOG2E) - lse_ref[h : h + 1, :] * LOG2E
+            s = dot_nn(kc_s[h], qt_s[qi, h])
+            zz = s * (scale * LOG2E) - lse_s[qi, h : h + 1, :] * LOG2E
             p = jnp.exp2(jnp.where(causal, zz, -1e30))
-            dp = dot_nn(v_s[:, h * VDIM : (h + 1) * VDIM], gt_s[h])
-            ds = (p * (dp - delta_s[h : h + 1, :])).astype(BF16)
+            dp = dot_nn(v_s[:, h * VDIM : (h + 1) * VDIM], gt_s[qi, h])
+            ds = (p * (dp - delta_s[qi, h : h + 1, :])).astype(BF16)
             dv_s[:, h * VDIM : (h + 1) * VDIM] = dot_nn(
-                p.astype(BF16), g_v[:, h * VDIM : (h + 1) * VDIM]
+                p.astype(BF16), g_v[qi, :, h * VDIM : (h + 1) * VDIM]
             ).astype(BF16)
-            dk = scale * dot_nn(ds, qs_s[h])
+            dk = scale * dot_nn(ds, qs_s[qi, h])
             dk_s[:, h * NOPE : (h + 1) * NOPE] = dk[:, :NOPE].astype(BF16)
             rope_sum = rope_sum + dk[:, NOPE:]
-            dqt_s[h] += dot_nn(kct_s[h], ds)
+            dqt_s[qi, h] += dot_nn(kct_s[h], ds)
             if h == 0:
 
                 @pl.when(n > 0)
@@ -388,13 +472,19 @@
         def _():
             stage_a(n + 2, 0)
 
-        @pl.when(jnp.logical_and(x == 0, n == lax.min(2, last)))
+        @pl.when(jnp.logical_and(jnp.logical_and(x == 0, z > 0), n == 2))
         def _():
             x_copy(i, 1).start()
 
         return carry
 
     lax.fori_loop(0, last + 1, slot, 0)
+
+    @pl.when(is_low)
+    def _():
+        for h in range(heads):
+            fq_v[:, h * width : (h + 1) * width] = (scale * dqt_s[1, h]).T[:, :width].astype(BF16)
+        back_copy().start()
 
     def dv_copy(d):
         k = (i + d) % ns
@@ -421,9 +511,6 @@
     def _():
         stage_r3(last - 1)
 
-    for h in range(heads):
-        dq_ref[:, h * width : (h + 1) * width] = (scale * dqt_s[h]).T[:, :width].astype(BF16)
-
     stage_r3(last)
 
     def tail(n, carry):
@@ -431,6 +518,22 @@
         return carry
 
     lax.fori_loop(lax.max(last - 2, 1), lower + 1, tail, 0)
+
+    @pl.when(jnp.logical_not(is_top))
+    def _():
+        for h in range(heads):
+            dq_ref[:, h * width : (h + 1) * width] = (
+                (scale * dqt_s[0, h]).T[:, :width].astype(BF16)
+            )
+
+    @pl.when(is_top)
+    def _():
+        back_copy().wait_recv()
+        for h in range(heads):
+            dq_ref[:, h * width : (h + 1) * width] = (
+                (scale * dqt_s[0, h]).T[:, :width]
+                + fq_v[:, h * width : (h + 1) * width].astype(F32)
+            ).astype(BF16)
 
     dvw = dvw_acc[pl.ds(pl.multiple_of(i * lrows, lrows), lrows), :]
     for d in range(1, ns):
@@ -447,7 +550,11 @@
     def _():
         add(z, 0)
 
-    lax.fori_loop(z + 1, nz, add, 0)
+    @pl.when(is_low)
+    def _():
+        add(nz, 0)
+
+    lax.fori_loop(z + 1, lax.select(is_low, jnp.int32(top), jnp.int32(nz)), add, 0)
     fin[pl.ds(my_piece, piece), :] = own_acc[...].astype(BF16)
 
     def ag_y(d):
@@ -485,19 +592,32 @@
         z_copy(i, 0).wait_send()
         z_copy(i, 1).wait_send()
 
-    @pl.when(x == 0)
+    @pl.when(jnp.logical_or(x == 0, is_low))
     def _():
         x_copy(i, 0).wait_send()
         x_copy(i, 1).wait_send()
 
+    @pl.when(is_top)
+    def _():
+        for k in range(4):
+            visit_copy(k).wait_send()
+
+    @pl.when(is_low)
+    def _():
+        back_copy().wait_send()
+
     def drain(n, carry):
-        @pl.when(jnp.logical_or(own_column(n), n > lower))
+        @pl.when(jnp.logical_or(own_column(n), in_plane(n)))
         def _():
             o_copy(n).wait_send()
 
-        @pl.when(jnp.logical_and(other_column(n), n <= lower))
+        @pl.when(for_x_sum(n))
         def _():
             xr_copy(n).wait_send()
+
+        @pl.when(visit_out(n))
+        def _():
+            v_copy(n).wait_send()
 
         return carry
 
@@ -540,15 +660,17 @@
         ],
         scratch_shapes=[
             pltpu.VMEM(queries.shape, BF16),
-            pltpu.VMEM(out_grad.shape, BF16),
+            pltpu.VMEM((2,) + out_grad.shape, BF16),
+            pltpu.VMEM(queries.shape, BF16),
+            pltpu.VMEM((2, heads, rows), F32),
             pltpu.VMEM(attn_out.shape, BF16),
             pltpu.VMEM(key_weight.shape, BF16),
             pltpu.VMEM(value_weight.shape, BF16),
-            pltpu.VMEM((heads, rows, WIDE), BF16),
-            pltpu.VMEM((heads, WIDE, rows), BF16),
-            pltpu.VMEM((heads, VDIM, rows), BF16),
-            pltpu.VMEM((heads, WIDE, rows), F32),
-            pltpu.VMEM((heads, rows), F32),
+            pltpu.VMEM((2, heads, rows, WIDE), BF16),
+            pltpu.VMEM((2, heads, WIDE, rows), BF16),
+            pltpu.VMEM((2, heads, VDIM, rows), BF16),
+            pltpu.VMEM((2, heads, WIDE, rows), F32),
+            pltpu.VMEM((2, heads, rows), F32),
             pltpu.VMEM((heads, rows, WIDE), BF16),
             pltpu.VMEM((heads, WIDE, rows), BF16),
             pltpu.VMEM((rows, hv), BF16),
@@ -561,7 +683,7 @@
             pltpu.VMEM((ns, rows // 2, packed), BF16),
             pltpu.VMEM((ns, max(ny - 1, 1), rows // tp, packed), BF16),
             pltpu.VMEM((ns, rows // tp, packed), BF16),
-            pltpu.VMEM((ns // 2, rows // tp, packed), BF16),
+            pltpu.VMEM((ns // 2 + 1, rows // tp, packed), BF16),
             pltpu.VMEM((rows // tp, packed), F32),
             pltpu.VMEM((rows, packed), BF16),
             dma((7,)),
@@ -577,7 +699,7 @@
             dma((ns,)),
             dma((ns, max(ny - 1, 1))),
             dma((ns, max(ny - 1, 1))),
-            dma((ns // 2,)),
+            dma((ns // 2 + 1,)),
             dma((ns,)),
             dma((ns,)),
             dma((ns,)),
@@ -585,6 +707,8 @@
             dma((max(ny - 1, 1),)),
             dma((1,)),
             dma((1,)),
+            dma((5,)),
+            dma((5,)),
         ],
         compiler_params=pltpu.CompilerParams(
             collective_id=0, has_side_effects=True, vmem_limit_bytes=67043328

time: 149 us -> 128 us (0.86)
  Pallas kernels: 140 us -> 119 us
    pallas_call x1, Pallas kernels: 140 us -> 119 us  [fused_backward(): pl.pallas_call(functools.partial(fused_kernel, ns, tp, heads, latent_dim)...]
where the time goes in v3:
time: 128 us
  Pallas kernels  119 us (93%)
  local copies, waits for them, and re-layouts  4.01 us (3%)
  other arithmetic  3.83 us (3%)
    pallas_call x1, Pallas kernels, fused_backward(): pl.pallas_call(functools.partial(fused_kernel, ns, tp, heads, latent_dim)...  119 us
    unnamed x8, local copies, waits for them, and re-layouts  3.32 us
    convert_element_type x1, other arithmetic, per_device(): d_latent = dlat.astype(F32)  2.83 us

profile of v3, /device:TPU:3, one launch (start us, length us, event | category | flops | bytes accessed | tf_op | source)
XLA Modules:
  0.0 127.9 jit_solution(16087214264901255671)
XLA Ops:
  0.6 1.0 copy.12
  1.6 0.7 pad.4.rope_hbm
  2.3 119.4 %shard_map.111 = (bf16[512,768]{1,0:T(8,128)(2,1)}, bf16[512,1024]{1,0:T(8,128)(2,1)}, bf16[512,128]{1,0:T(8,128)(2,1)}, f32[128,512]{1,0:T(8,128)}) custom-call(bf16[512,768]{1,0:T(8,128)(2,1)} %q_hbm.1, bf16[512,512]{1,0:T(8,128)(2,1)} %g_hbm.1, bf16[512,512]{1,0:T(8,128)(2,1)} %ao_hbm.1, f32[4,512]{1,0:T(4,128)} %lse_ref.1, bf16[512,1024]{1,0:T(8,128)(2,1)} %lat_hbm.1, ...), custom_call_target="tpu_custom_call" | custom-call | tf_op jit(solution)/shard_map/pallas_call | solution.py:651
  121.7 0.0 copy-start
  121.7 1.0 slice_convert_fusion
  122.7 0.8 copy.13
  123.5 0.0 copy-start.1
  123.5 2.8 %convert_element_type.8 = f32[512,1024]{1,0:T(8,128)} convert(bf16[512,1024]{1,0:T(8,128)(2,1)} %get-tuple-element.9) | non-fusion elementwise | flops 524288 | bytes 3145728 | tf_op jit(solution)/shard_map/convert_element_type | solution.py:725
  126.3 0.0 copy-done
  126.3 0.9 copy.16
  127.2 0.0 copy-done.1
  127.2 0.7 copy.17
Async XLA Ops:
  121.7 4.6 %copy-start = (bf16[512,768]{1,0:T(8,128)(2,1)S(1)}, bf16[512,768]{1,0:T(8,128)(2,1)}, u32[]{:S(2)}) copy-start(bf16[512,768]{1,0:T(8,128)(2,1)} %get-tuple-element.20) | copy-start | bytes 2359300
  123.5 3.7 %copy-start.1 = (f32[128,512]{1,0:T(8,128)S(1)}, f32[128,512]{1,0:T(8,128)}, u32[]{:S(2)}) copy-start(f32[128,512]{1,0:T(8,128)} %get-tuple-element.23) | copy-start | bytes 786436

commit v4 on v3

--- a/solution.py
+++ b/solution.py
@@ -35,12 +35,12 @@
     ao_hbm,
     lse_ref,
     lat_hbm,
-    rope_hbm,
+    rope_ref,
     wk_hbm,
     wv_hbm,
     dq_ref,
     dlat_hbm,
-    drope_hbm,
+    drope_ref,
     dvw_ref,
     q_v,
     g_v,
@@ -61,6 +61,7 @@
     dv_s,
     dvw_acc,
     dvw_b,
+    dvx_rx,
     dvw_rx,
     lat_all,
     crx,
@@ -86,6 +87,8 @@
     ors,
     dvr,
     dvs,
+    dvxr,
+    dvxs,
     agr,
     ags,
     acr,
@@ -103,6 +106,8 @@
     half, quart, piece = rows // 2, rows // 4, rows // tp
     scale = width ** (-0.5)
     lrows = latent_dim // ns
+    chunks = yr.shape[2]
+    sub = piece // chunks
 
     top = nz - 1
     is_top, is_low = z == top, z == 0
@@ -155,10 +160,7 @@
     def lat_rows(j, at, size):
         return lat_all.at[j, pl.ds(at, size)]
 
-    own_cps = [
-        pltpu.make_async_copy(lat_hbm, lat_all.at[i, :, pl.ds(0, latent_dim)], ld.at[0]),
-        pltpu.make_async_copy(rope_hbm, lat_all.at[i, :, pl.ds(latent_dim, WIDE - NOPE)], ld.at[6]),
-    ]
+    own_cps = [pltpu.make_async_copy(lat_hbm, lat_all.at[i, :, pl.ds(0, latent_dim)], ld.at[0])]
     loads = [
         pltpu.make_async_copy(s, d, ld.at[k + 1])
         for k, (s, d) in enumerate(
@@ -168,6 +170,10 @@
     for cp in own_cps + loads:
         cp.start()
 
+    lat_all[i, :, latent_dim:] = jnp.concatenate(
+        [rope_ref[...].T, jnp.zeros((rows, WIDE - NOPE - ROPE), BF16)], axis=1
+    )
+
     barrier = pltpu.get_barrier_semaphore()
     for d in range(1, ns):
         pl.semaphore_signal(
@@ -267,90 +273,112 @@
             lat_rows(part_of(n), peer_half, half), crx.at[j], r1s.at[j], r1r.at[j], core_peer
         )
 
-    def y_copy(n, d):
+    def rows_of(yy, k):
+        return pl.ds(pl.multiple_of(c * half + yy * piece + k * sub, sub), sub)
+
+    def chunk(k):
+        return pl.ds(k * sub, sub)
+
+    def y_copy(n, d, k):
         j = key_of(n)
         yy = (y + d) % ny
-        at = pl.multiple_of(c * half + yy * piece, piece)
         return remote(
-            lat_rows(part_of(n), at, piece), yrx.at[j, d - 1], ys.at[j, d - 1], yr.at[j, d - 1],
-            {"sp": i, "tp": yy * 2 + c},
-        )
-
-    my_piece = pl.multiple_of(c * half + y * piece, piece)
-
-    def xr_copy(n):
+            lat_all.at[part_of(n), rows_of(yy, k)], yrx.at[j, d - 1, chunk(k)],
+            ys.at[j, d - 1, k], yr.at[j, d - 1, k], {"sp": i, "tp": yy * 2 + c},
+        )
+
+    def xr_copy(n, k):
         j = block_of(n)
-        return remote(lat_rows(part_of(n), my_piece, piece), xrx.at[j], xrs.at[j], xrr.at[j], x_peer)
-
-    def o_copy(n):
         return remote(
-            lat_rows(part_of(n), my_piece, piece), orx.at[z], ors.at[key_of(n)], orr.at[z],
+            lat_all.at[part_of(n), rows_of(y, k)], xrx.at[j, chunk(k)], xrs.at[j, k], xrr.at[j, k], x_peer
+        )
+
+    def o_copy(n, k):
+        return remote(
+            lat_all.at[part_of(n), rows_of(y, k)], orx.at[z, chunk(k)], ors.at[key_of(n), k], orr.at[z, k],
             {"sp": block_of(n), "tp": t},
         )
 
-    def v_copy(n):
+    def v_copy(n, k):
         return remote(
-            lat_rows(part_of(n), my_piece, piece), orx.at[nz], ors.at[key_of(n)], orr.at[nz], x_peer
-        )
-
-    def o_wait(zz):
+            lat_all.at[part_of(n), rows_of(y, k)], orx.at[nz, chunk(k)], ors.at[key_of(n), k],
+            orr.at[nz, k], x_peer,
+        )
+
+    def o_wait(zz, k):
         return remote(
-            lat_rows(i, my_piece, piece), orx.at[zz], ors.at[i], orr.at[zz], x_peer
+            lat_all.at[i, rows_of(y, k)], orx.at[zz, chunk(k)], ors.at[i, k], orr.at[zz, k], x_peer
         )
 
     def stage_r2(n):
         j = key_of(n)
         b = part_of(n)
         r1_copy(n).wait_recv()
-        mine = lat_all[b, pl.ds(my_half, half), :].astype(F32)
-        lat_all[b, pl.ds(my_half, half), :] = (mine + crx[j].astype(F32)).astype(BF16)
-        for d in range(1, ny):
-            y_copy(n, d).start()
+
+        def add_core(yy, k):
+            at = pl.ds(pl.multiple_of(yy * piece + k * sub, sub), sub)
+            lat_all[b, rows_of(yy, k), :] = (
+                lat_all[b, rows_of(yy, k), :].astype(F32) + crx[j, at, :].astype(F32)
+            ).astype(BF16)
+
+        for k in range(chunks):
+            for d in range(1, ny):
+                add_core((y + d) % ny, k)
+                y_copy(n, d, k).start()
+        for k in range(chunks):
+            add_core(y, k)
 
     def stage_r3(n):
         j = key_of(n)
         b = part_of(n)
-        total = lat_all[b, pl.ds(my_piece, piece), :].astype(F32)
-        for d in range(1, ny):
-            y_copy(n, d).wait_recv()
-            total = total + yrx[j, d - 1].astype(F32)
-        for d in range(1, ny):
-            y_copy(n, d).wait_send()
+        for k in range(chunks):
+            total = lat_all[b, rows_of(y, k), :].astype(F32)
+            for d in range(1, ny):
+                y_copy(n, d, k).wait_recv()
+                total = total + yrx[j, d - 1, k * sub : (k + 1) * sub, :].astype(F32)
+
+            @pl.when(n == 0)
+            def _():
+                own_acc[k * sub : (k + 1) * sub, :] = total
+
+            @pl.when(jnp.logical_and(is_low, n == base + 1))
+            def _():
+                own_acc[k * sub : (k + 1) * sub, :] += total
+
+            @pl.when(n > 0)
+            def _():
+                lat_all[b, rows_of(y, k), :] = total.astype(BF16)
+
+            @pl.when(for_x_sum(n))
+            def _():
+                xr_copy(n, k).start()
+
+            @pl.when(in_plane(n))
+            def _():
+                o_copy(n, k).start()
+
+            @pl.when(visit_out(n))
+            def _():
+                v_copy(n, k).start()
+
+        for k in range(chunks):
+            for d in range(1, ny):
+                y_copy(n, d, k).wait_send()
         r1_copy(n).wait_send()
-
-        @pl.when(n == 0)
-        def _():
-            own_acc[...] = total
-
-        @pl.when(jnp.logical_and(is_low, n == base + 1))
-        def _():
-            own_acc[...] += total
-
-        @pl.when(n > 0)
-        def _():
-            lat_all[b, pl.ds(my_piece, piece), :] = total.astype(BF16)
-
-        @pl.when(for_x_sum(n))
-        def _():
-            xr_copy(n).start()
-
-        @pl.when(in_plane(n))
-        def _():
-            o_copy(n).start()
-
-        @pl.when(visit_out(n))
-        def _():
-            v_copy(n).start()
 
     def stage_r4(n):
         @pl.when(own_column(n))
         def _():
             j = block_of(n)
             b = part_of(n)
-            xr_copy(n).wait_recv()
-            total = lat_all[b, pl.ds(my_piece, piece), :].astype(F32) + xrx[j].astype(F32)
-            lat_all[b, pl.ds(my_piece, piece), :] = total.astype(BF16)
-            o_copy(n).start()
+            for k in range(chunks):
+                xr_copy(n, k).wait_recv()
+                total = (
+                    lat_all[b, rows_of(y, k), :].astype(F32)
+                    + xrx[j, k * sub : (k + 1) * sub, :].astype(F32)
+                )
+                lat_all[b, rows_of(y, k), :] = total.astype(BF16)
+                o_copy(n, k).start()
 
     def prepare(qi, q_ref):
         for h in range(heads):
@@ -437,12 +465,9 @@
                 @pl.when(n > 1)
                 def _():
                     stage_a(n + 1, 1)
+                    stage_r3(n - 2)
 
             if h == heads // 2:
-
-                @pl.when(n > 1)
-                def _():
-                    stage_r3(n - 2)
 
                 @pl.when(n == 0)
                 def _():
@@ -486,20 +511,27 @@
             fq_v[:, h * width : (h + 1) * width] = (scale * dqt_s[1, h]).T[:, :width].astype(BF16)
         back_copy().start()
 
+    def wrows(k):
+        return pl.ds(pl.multiple_of(k * lrows, lrows), lrows)
+
+    def dvx_copy():
+        return remote(dvw_b.at[1 - x], dvx_rx, dvxs.at[0], dvxr.at[0], x_peer)
+
     def dv_copy(d):
-        k = (i + d) % ns
+        zz = (z + d) % nz
         return remote(
-            dvw_b.at[k], dvw_rx.at[ns - d], dvs.at[d], dvr.at[ns - d], {"sp": k, "tp": t}
+            dvw_b.at[x, zz], dvw_rx.at[nz - d], dvs.at[d], dvr.at[nz - d], {"sp": 2 * zz + x, "tp": t}
         )
 
     def dv_wait(d):
-        k = (i + d) % ns
-        return remote(dvw_b.at[k], dvw_rx.at[d], dvs.at[d], dvr.at[d], {"sp": k, "tp": t})
+        return remote(dvw_b.at[x, z], dvw_rx.at[d], dvs.at[d], dvr.at[d], x_peer)
 
     for k in range(ns):
-        dvw_b[k] = dvw_acc[k * lrows : (k + 1) * lrows, :].astype(BF16)
-    for d in range(1, ns):
-        dv_copy(d).start()
+        dvw_b[k % 2, k // 2] = dvw_acc[k * lrows : (k + 1) * lrows, :].astype(BF16)
+
+    @pl.when(x == 0)
+    def _():
+        dvx_copy().start()
 
     stage_r2(last)
 
@@ -511,13 +543,9 @@
     def _():
         stage_r3(last - 1)
 
-    stage_r3(last)
-
-    def tail(n, carry):
-        stage_r4(n)
-        return carry
-
-    lax.fori_loop(lax.max(last - 2, 1), lower + 1, tail, 0)
+    @pl.when(x == 1)
+    def _():
+        dvx_copy().start()
 
     @pl.when(jnp.logical_not(is_top))
     def _():
@@ -525,6 +553,20 @@
             dq_ref[:, h * width : (h + 1) * width] = (
                 (scale * dqt_s[0, h]).T[:, :width].astype(BF16)
             )
+
+    stage_r3(last)
+
+    def tail(n, carry):
+        stage_r4(n)
+        return carry
+
+    lax.fori_loop(lax.max(last - 2, 1), lower + 1, tail, 0)
+    dvx_copy().wait_recv()
+    dvx_copy().wait_send()
+    for d in range(1, nz):
+        zz = (z + d) % nz
+        dvw_b[x, zz] = (dvw_acc[wrows(2 * zz + x), :] + dvx_rx[zz].astype(F32)).astype(BF16)
+        dv_copy(d).start()
 
     @pl.when(is_top)
     def _():
@@ -535,46 +577,48 @@
                 + fq_v[:, h * width : (h + 1) * width].astype(F32)
             ).astype(BF16)
 
-    dvw = dvw_acc[pl.ds(pl.multiple_of(i * lrows, lrows), lrows), :]
-    for d in range(1, ns):
+    def ag_y(d, k):
+        yy = (y + d) % ny
+        return remote(
+            fin.at[rows_of(y, k)], fin.at[rows_of(y, k)], ags.at[d - 1, k], agr.at[d - 1, k],
+            {"sp": i, "tp": yy * 2 + c},
+        )
+
+    def ag_y_wait(d, k):
+        yy = (y + ny - d) % ny
+        return remote(
+            fin.at[rows_of(yy, k)], fin.at[rows_of(yy, k)], ags.at[d - 1, k], agr.at[d - 1, k],
+            {"sp": i, "tp": yy * 2 + c},
+        )
+
+    for k in range(chunks):
+
+        def add(zz, carry):
+            o_wait(zz, k).wait_recv()
+            own_acc[k * sub : (k + 1) * sub, :] += orx[zz, k * sub : (k + 1) * sub, :].astype(F32)
+            return carry
+
+        @pl.when(x == 0)
+        def _():
+            add(z, 0)
+
+        @pl.when(is_low)
+        def _():
+            add(nz, 0)
+
+        lax.fori_loop(z + 1, lax.select(is_low, jnp.int32(top), jnp.int32(nz)), add, 0)
+        fin[rows_of(y, k), :] = own_acc[k * sub : (k + 1) * sub, :].astype(BF16)
+        for d in range(1, ny):
+            ag_y(d, k).start()
+
+    dvw = dvw_acc[wrows(i), :] + dvx_rx[z].astype(F32)
+    for d in range(1, nz):
         dv_wait(d).wait_recv()
         dvw = dvw + dvw_rx[d].astype(F32)
     dvw_ref[...] = dvw
-
-    def add(k, carry):
-        o_wait(k).wait_recv()
-        own_acc[...] += orx[k].astype(F32)
-        return carry
-
-    @pl.when(x == 0)
-    def _():
-        add(z, 0)
-
-    @pl.when(is_low)
-    def _():
-        add(nz, 0)
-
-    lax.fori_loop(z + 1, lax.select(is_low, jnp.int32(top), jnp.int32(nz)), add, 0)
-    fin[pl.ds(my_piece, piece), :] = own_acc[...].astype(BF16)
-
-    def ag_y(d):
-        yy = (y + d) % ny
-        return remote(
-            fin.at[pl.ds(my_piece, piece)], fin.at[pl.ds(my_piece, piece)], ags.at[d - 1], agr.at[d - 1],
-            {"sp": i, "tp": yy * 2 + c},
-        )
-
-    def ag_y_wait(d):
-        at = pl.multiple_of(c * half + ((y + ny - d) % ny) * piece, piece)
-        return remote(
-            fin.at[pl.ds(at, piece)], fin.at[pl.ds(at, piece)], ags.at[d - 1], agr.at[d - 1],
-            {"sp": i, "tp": ((y + ny - d) % ny) * 2 + c},
-        )
-
-    for d in range(1, ny):
-        ag_y(d).start()
-    for d in range(1, ny):
-        ag_y_wait(d).wait_recv()
+    for k in range(chunks):
+        for d in range(1, ny):
+            ag_y_wait(d, k).wait_recv()
     ag_c = remote(
         fin.at[pl.ds(my_half, half)], fin.at[pl.ds(my_half, half)], acs.at[0], acr.at[0], core_peer
     )
@@ -583,6 +627,13 @@
     )
     ag_c.start()
 
+    def out_copy(at, k):
+        return pltpu.make_async_copy(
+            fin.at[pl.ds(at, half), pl.ds(0, latent_dim)], dlat_hbm.at[pl.ds(at, half)], ld.at[k]
+        )
+
+    out_copy(my_half, 0).start()
+
     @pl.when(last > 0)
     def _():
         sends_done(last)
@@ -609,53 +660,54 @@
     def drain(n, carry):
         @pl.when(jnp.logical_or(own_column(n), in_plane(n)))
         def _():
-            o_copy(n).wait_send()
+            for k in range(chunks):
+                o_copy(n, k).wait_send()
 
         @pl.when(for_x_sum(n))
         def _():
-            xr_copy(n).wait_send()
+            for k in range(chunks):
+                xr_copy(n, k).wait_send()
 
         @pl.when(visit_out(n))
         def _():
-            v_copy(n).wait_send()
+            for k in range(chunks):
+                v_copy(n, k).wait_send()
 
         return carry
 
     lax.fori_loop(1, last + 1, drain, 0)
-    for d in range(1, ns):
+    for d in range(1, nz):
         dv_copy(d).wait_send()
-    for d in range(1, ny):
-        ag_y(d).wait_send()
+    for k in range(chunks):
+        for d in range(1, ny):
+            ag_y(d, k).wait_send()
     ag_c_wait.wait_recv()
     ag_c.wait_send()
-    outs = [
-        pltpu.make_async_copy(fin.at[:, pl.ds(0, latent_dim)], dlat_hbm, ld.at[0]),
-        pltpu.make_async_copy(fin.at[:, pl.ds(latent_dim, WIDE - NOPE)], drope_hbm, ld.at[6]),
-    ]
-    for out in outs:
-        out.start()
-    for out in outs:
-        out.wait()
-
-
-def fused_backward(ns, tp, queries, out_grad, attn_out, lse, latent, rope, key_weight, value_weight):
+    out_copy(peer_half, 1).start()
+    drope_ref[...] = fin[:, latent_dim : latent_dim + ROPE].astype(F32).T
+    out_copy(my_half, 0).wait()
+    out_copy(peer_half, 1).wait()
+
+
+def fused_backward(ns, tp, queries, out_grad, attn_out, lse, latent, rope_t, key_weight, value_weight):
     rows = queries.shape[0]
     latent_dim, hv = key_weight.shape
     heads = hv // NOPE
-    packed = latent_dim + rope.shape[1]
+    packed = latent_dim + WIDE - NOPE
     lrows = latent_dim // ns
     ny = tp // 2
+    chunks = min(4, rows // tp // 32)
     hbm = pl.BlockSpec(memory_space=pl.ANY)
     vmem = pl.BlockSpec(memory_space=pltpu.VMEM)
     dma = pltpu.SemaphoreType.DMA
     return pl.pallas_call(
         functools.partial(fused_kernel, ns, tp, heads, latent_dim),
-        in_specs=[hbm, hbm, hbm, vmem, hbm, hbm, hbm, hbm],
-        out_specs=[vmem, hbm, hbm, vmem],
+        in_specs=[hbm, hbm, hbm, vmem, hbm, vmem, hbm, hbm],
+        out_specs=[vmem, hbm, vmem, vmem],
         out_shape=[
             jax.ShapeDtypeStruct(queries.shape, BF16),
             jax.ShapeDtypeStruct(latent.shape, BF16),
-            jax.ShapeDtypeStruct(rope.shape, BF16),
+            jax.ShapeDtypeStruct(rope_t.shape, F32),
             jax.ShapeDtypeStruct((lrows, hv), F32),
         ],
         scratch_shapes=[
@@ -677,8 +729,9 @@
             pltpu.VMEM((rows, hv), BF16),
             pltpu.VMEM((rows, hv), BF16),
             pltpu.VMEM((latent_dim, hv), F32),
-            pltpu.VMEM((ns, lrows, hv), BF16),
-            pltpu.VMEM((ns, lrows, hv), BF16),
+            pltpu.VMEM((2, ns // 2, lrows, hv), BF16),
+            pltpu.VMEM((ns // 2, lrows, hv), BF16),
+            pltpu.VMEM((ns // 2, lrows, hv), BF16),
             pltpu.VMEM((ns + 2, rows, packed), BF16),
             pltpu.VMEM((ns, rows // 2, packed), BF16),
             pltpu.VMEM((ns, max(ny - 1, 1), rows // tp, packed), BF16),
@@ -686,25 +739,27 @@
             pltpu.VMEM((ns // 2 + 1, rows // tp, packed), BF16),
             pltpu.VMEM((rows // tp, packed), F32),
             pltpu.VMEM((rows, packed), BF16),
-            dma((7,)),
+            dma((6,)),
             dma((ns, 2)),
             dma((ns, 2)),
             dma((ns, 2)),
             dma((ns, 2)),
             dma((ns,)),
             dma((ns,)),
+            dma((ns, chunks)),
+            dma((ns, chunks)),
             dma((ns,)),
             dma((ns,)),
-            dma((ns,)),
-            dma((ns,)),
-            dma((ns, max(ny - 1, 1))),
-            dma((ns, max(ny - 1, 1))),
-            dma((ns // 2 + 1,)),
-            dma((ns,)),
-            dma((ns,)),
-            dma((ns,)),
-            dma((max(ny - 1, 1),)),
-            dma((max(ny - 1, 1),)),
+            dma((ns, max(ny - 1, 1), chunks)),
+            dma((ns, max(ny - 1, 1), chunks)),
+            dma((ns // 2 + 1, chunks)),
+            dma((ns, chunks)),
+            dma((ns // 2,)),
+            dma((ns // 2,)),
+            dma((1,)),
+            dma((1,)),
+            dma((max(ny - 1, 1), chunks)),
+            dma((max(ny - 1, 1), chunks)),
             dma((1,)),
             dma((1,)),
             dma((5,)),
@@ -713,17 +768,16 @@
         compiler_params=pltpu.CompilerParams(
             collective_id=0, has_side_effects=True, vmem_limit_bytes=67043328
         ),
-    )(queries, out_grad, attn_out, lse, latent, rope, key_weight, value_weight)
+    )(queries, out_grad, attn_out, lse, latent, rope_t, key_weight, value_weight)
 
 
 def per_device(queries, latent, rope_key, key_weight, value_weight, log_sums, attn_out, out_grad):
-    rope = jnp.pad(rope_key, ((0, 0), (0, WIDE - NOPE - ROPE)))
-    d_queries, dlat, drope, d_value_weight = fused_backward(
+    d_queries, dlat, drope_t, d_value_weight = fused_backward(
         lax.axis_size("sp"), lax.axis_size("tp"),
-        queries, out_grad, attn_out, log_sums, latent, rope, key_weight, value_weight,
+        queries, out_grad, attn_out, log_sums, latent, rope_key.T, key_weight, value_weight,
     )
     d_latent = dlat.astype(F32)
-    d_rope = drope[:, :ROPE].astype(F32)
+    d_rope = drope_t.T
     return (d_queries, d_latent, d_rope, d_value_weight)
 
 

time: 128 us -> 111 us (0.87)
  the two profiles are of different devices: /device:TPU:3 before, /device:TPU:0 now
where the time goes in v4:
time: 111 us; the launch traced here: 108 us
  Pallas kernels  103 us (93%)
  other arithmetic  2.88 us (3%)
  local copies, waits for them, and re-layouts  2.25 us (2%)
    pallas_call x1, Pallas kernels, fused_backward(): pl.pallas_call(functools.partial(fused_kernel, ns, tp, heads, latent_dim)...  103 us
    convert_element_type x1, other arithmetic, per_device(): d_latent = dlat.astype(F32)  2.88 us
    unnamed x9, local copies, waits for them, and re-layouts  2.25 us

profile of v4, /device:TPU:0, one launch (start us, length us, event | category | flops | bytes accessed | tf_op | source)
XLA Modules:
  0.0 108.5 jit_solution(4708956052014076281)
XLA Ops:
  0.6 102.7 %shard_map.111 = (bf16[512,768]{1,0:T(8,128)(2,1)}, bf16[512,1024]{1,0:T(8,128)(2,1)}, f32[64,512]{1,0:T(8,128)}, f32[128,512]{1,0:T(8,128)}) custom-call(bf16[512,768]{1,0:T(8,128)(2,1)} %q_hbm.1, bf16[512,512]{1,0:T(8,128)(2,1)} %g_hbm.1, bf16[512,512]{1,0:T(8,128)(2,1)} %ao_hbm.1, f32[4,512]{1,0:T(4,128)} %lse_ref.1, bf16[512,1024]{1,0:T(8,128)(2,1)} %lat_hbm.1, ...), custom_call_target="tpu_custom_call" | custom-call | tf_op jit(solution)/shard_map/pallas_call | solution.py:703
  103.3 0.0 copy-start
  103.3 0.0 copy-start.2
  103.3 0.0 copy-start.1
  103.3 2.9 %convert_element_type.3 = f32[512,1024]{1,0:T(8,128)} convert(bf16[512,1024]{1,0:T(8,128)(2,1)} %get-tuple-element.9) | non-fusion elementwise | flops 524288 | bytes 3145728 | tf_op jit(solution)/shard_map/convert_element_type | solution.py:779
  106.2 0.0 copy-done
  106.2 0.9 copy.15
  107.1 0.0 copy-done.2
  107.1 0.7 copy.16
  107.8 0.0 copy-done.1
  107.8 0.7 copy.17
Async XLA Ops:
  103.3 2.9 %copy-start = (bf16[512,768]{1,0:T(8,128)(2,1)S(1)}, bf16[512,768]{1,0:T(8,128)(2,1)}, u32[]{:S(2)}) copy-start(bf16[512,768]{1,0:T(8,128)(2,1)} %get-tuple-element.16) | copy-start | bytes 2359300
  103.3 3.8 %copy-start.2 = (f32[64,512]{1,0:T(8,128)S(1)}, f32[64,512]{1,0:T(8,128)}, u32[]{:S(2)}) copy-start(f32[64,512]{1,0:T(8,128)} %get-tuple-element.10) | copy-start | bytes 393220
  103.3 4.4 %copy-start.1 = (f32[128,512]{1,0:T(8,128)S(1)}, f32[128,512]{1,0:T(8,128)}, u32[]{:S(2)}) copy-start(f32[128,512]{1,0:T(8,128)} %get-tuple-element.19) | copy-start | bytes 786436

commit v5 on v4

--- a/solution.py
+++ b/solution.py
@@ -38,7 +38,7 @@
     rope_ref,
     wk_hbm,
     wv_hbm,
-    dq_ref,
+    dq_hbm,
     dlat_hbm,
     drope_ref,
     dvw_ref,
@@ -56,6 +56,7 @@
     delta_s,
     kc_s,
     kct_s,
+    lat_t,
     v_s,
     dk_s,
     dv_s,
@@ -103,7 +104,10 @@
     z, x = i // 2, i % 2
     y, c = t // 2, t % 2
     rows, width = q_v.shape[0], NOPE + ROPE
-    half, quart, piece = rows // 2, rows // 4, rows // tp
+    half, piece = rows // 2, rows // tp
+    parts = zr.shape[1]
+    bit = half // parts
+    early, late = range(parts // 2), range(parts // 2, parts)
     scale = width ** (-0.5)
     lrows = latent_dim // ns
     chunks = yr.shape[2]
@@ -187,32 +191,34 @@
     for cp in own_cps:
         cp.wait()
 
-    def quarter(j, k):
-        return lat_rows(j, pl.multiple_of(c * half + k * quart, quart), quart)
+    def bit_of(j, k):
+        return lat_rows(j, pl.multiple_of(c * half + k * bit, bit), bit)
 
     def z_copy(j, k):
-        return remote(quarter(j, k), quarter(j, k), zs.at[j, k], zr.at[j, k], above)
+        return remote(bit_of(j, k), bit_of(j, k), zs.at[j, k], zr.at[j, k], above)
 
     def x_copy(j, k):
-        return remote(quarter(j, k), quarter(j, k), xs.at[j, k], xr.at[j, k], x_peer)
-
-    def c_copy(j):
-        return remote(lat_rows(j, my_half, half), lat_rows(j, my_half, half), cs.at[j], cr.at[j], core_peer)
+        return remote(bit_of(j, k), bit_of(j, k), xs.at[j, k], xr.at[j, k], x_peer)
+
+    def c_copy(j, k):
+        return remote(bit_of(j, k), bit_of(j, k), cs.at[j, k], cr.at[j, k], core_peer)
 
     has_next = z + 1 < nz
 
     @pl.when(has_next)
     def _():
-        z_copy(i, 0).start()
-        z_copy(i, 1).start()
+        for k in range(parts):
+            z_copy(i, k).start()
 
     @pl.when(jnp.logical_or(x == 0, is_low))
     def _():
-        x_copy(i, 0).start()
+        for k in early:
+            x_copy(i, k).start()
 
     @pl.when(is_low)
     def _():
-        x_copy(i, 1).start()
+        for k in late:
+            x_copy(i, k).start()
 
     def goes_on(n):
         return jnp.logical_and(has_next, jnp.logical_or(z + 1 != top, block_of(n) >= 2))
@@ -228,43 +234,41 @@
     def back_copy():
         return remote(fq_v, fq_v, vs.at[4], vr.at[4], top_peer)
 
-    def stage_a(n, k):
+    def stage_a(n, pieces):
         @pl.when(own_column(n))
         def _():
             j = block_of(n)
-            z_copy(j, k).wait_recv()
-            x_copy(j, k).start()
-
-            @pl.when(goes_on(n))
-            def _():
-                z_copy(j, k).start()
-
-            if k == 1:
-                c_copy(j).start()
+            for k in pieces:
+                z_copy(j, k).wait_recv()
+                x_copy(j, k).start()
+                c_copy(j, k).start()
+
+                @pl.when(goes_on(n))
+                def _():
+                    z_copy(j, k).start()
 
     def stage_b(n):
-        @pl.when(by_x(n))
-        def _():
-            j = block_of(n)
-            x_copy(j, 0).wait_recv()
-            x_copy(j, 1).wait_recv()
-            c_copy(j).start()
+        j = block_of(n)
+        for k in range(parts):
+            x_copy(j, k).wait_recv()
+            c_copy(j, k).start()
 
     def sends_done(n):
         j = block_of(n)
 
         @pl.when(jnp.logical_or(own_column(n), by_x(n)))
         def _():
-            c_copy(j).wait_send()
+            for k in range(parts):
+                c_copy(j, k).wait_send()
 
         @pl.when(own_column(n))
         def _():
-            for k in range(2):
+            for k in range(parts):
                 x_copy(j, k).wait_send()
 
             @pl.when(goes_on(n))
             def _():
-                for k in range(2):
+                for k in range(parts):
                     z_copy(j, k).wait_send()
 
     def r1_copy(n):
@@ -317,9 +321,7 @@
 
         def add_core(yy, k):
             at = pl.ds(pl.multiple_of(yy * piece + k * sub, sub), sub)
-            lat_all[b, rows_of(yy, k), :] = (
-                lat_all[b, rows_of(yy, k), :].astype(F32) + crx[j, at, :].astype(F32)
-            ).astype(BF16)
+            lat_all[b, rows_of(yy, k), :] = lat_all[b, rows_of(yy, k), :] + crx[j, at, :]
 
         for k in range(chunks):
             for d in range(1, ny):
@@ -414,37 +416,43 @@
 
     dvw_acc[...] = jnp.zeros_like(dvw_acc)
 
-    def slot(n, carry):
+    def slot(n, diagonal):
         j = block_of(n)
         b = part_of(n)
         qi = lax.select(visiting(n), jnp.int32(1), jnp.int32(0))
-        q_block = lax.select(visiting(n), 2 * top + x, i)
-
-        @pl.when(jnp.logical_or(own_column(n), by_x(n)))
-        def _():
-            c_copy(j).wait_recv()
-
-        @pl.when(n == base + 1)
-        def _():
-            for k in range(4):
-                visit_copy(k).wait_recv()
-            prepare(1, fq_v)
+
+        if not diagonal:
+
+            @pl.when(jnp.logical_or(own_column(n), by_x(n)))
+            def _():
+                for k in range(parts):
+                    c_copy(j, k).wait_recv()
+
+            @pl.when(n == base + 1)
+            def _():
+                for k in range(4):
+                    visit_copy(k).wait_recv()
+                prepare(1, fq_v)
 
         rope = lat_all[j, :, latent_dim:]
+        rope_t = rope.T[:ROPE]
+        lat_t[...] = lat_all[j, :, :latent_dim].T
         keys = dot_nn(lat_all[j, :, :latent_dim], wk_v[...]).astype(BF16)
         v_s[...] = dot_nn(lat_all[j, :, :latent_dim], wv_v[...]).astype(BF16)
         for h in range(heads):
             kc = jnp.concatenate([keys[:, h * NOPE : (h + 1) * NOPE], rope], axis=1)
             kc_s[h] = kc
-            kct_s[h] = kc.T
+            kct_s[h, :NOPE] = keys[:, h * NOPE : (h + 1) * NOPE].T
+            kct_s[h, NOPE:] = rope_t
         rope_sum = jnp.zeros((rows, WIDE - NOPE), F32)
-        k_pos = lax.broadcasted_iota(jnp.int32, (rows, rows), 0)
-        q_pos = lax.broadcasted_iota(jnp.int32, (rows, rows), 1)
-        causal = k_pos - q_pos <= (q_block - j) * rows
         for h in range(heads):
             s = dot_nn(kc_s[h], qt_s[qi, h])
             zz = s * (scale * LOG2E) - lse_s[qi, h : h + 1, :] * LOG2E
-            p = jnp.exp2(jnp.where(causal, zz, -1e30))
+            if diagonal:
+                k_pos = lax.broadcasted_iota(jnp.int32, (rows, rows), 0)
+                q_pos = lax.broadcasted_iota(jnp.int32, (rows, rows), 1)
+                zz = jnp.where(k_pos <= q_pos, zz, -1e30)
+            p = jnp.exp2(zz)
             dp = dot_nn(v_s[:, h * VDIM : (h + 1) * VDIM], gt_s[qi, h])
             ds = (p * (dp - delta_s[qi, h : h + 1, :])).astype(BF16)
             dv_s[:, h * VDIM : (h + 1) * VDIM] = dot_nn(
@@ -454,68 +462,72 @@
             dk_s[:, h * NOPE : (h + 1) * NOPE] = dk[:, :NOPE].astype(BF16)
             rope_sum = rope_sum + dk[:, NOPE:]
             dqt_s[qi, h] += dot_nn(kct_s[h], ds)
-            if h == 0:
-
-                @pl.when(n > 0)
-                def _():
-                    stage_r2(n - 1)
-
-            if h == (heads - 1) // 2:
+            if h == heads // 2 - 1 and not diagonal:
+                stage_r2(n - 1)
 
                 @pl.when(n > 1)
                 def _():
-                    stage_a(n + 1, 1)
-                    stage_r3(n - 2)
-
-            if h == heads // 2:
-
-                @pl.when(n == 0)
+                    stage_a(n + 1, late)
+
+        if not diagonal:
+
+            @pl.when(n > 1)
+            def _():
+                stage_r3(n - 2)
+                sends_done(n - 1)
+
+                @pl.when(n > 4)
                 def _():
-                    stage_a(n + 1, 0)
-
-        @pl.when(n > 4)
-        def _():
-            stage_r4(n - 4)
-
-        @pl.when(n > 1)
-        def _():
-            sends_done(n - 1)
+                    stage_r4(n - 4)
+
+                @pl.when(in_plane(n + 1))
+                def _():
+                    stage_b(n + 1)
 
         dlat = dot_nt(dk_s[...], wk_v[...]) + dot_nt(dv_s[...], wv_v[...])
         lat_all[b, :, :latent_dim] = dlat.astype(BF16)
         lat_all[b, :, latent_dim:] = rope_sum.astype(BF16)
         r1_copy(n).start()
 
-        @pl.when(n == 0)
-        def _():
-            stage_a(n + 1, 1)
-
-        stage_b(n + 1)
-        dvw_acc[...] += dot_nn(lat_all[j, :, :latent_dim].T, dv_s[...])
-
-        @pl.when(n > 0)
-        def _():
-            stage_a(n + 2, 0)
-
-        @pl.when(jnp.logical_and(jnp.logical_and(x == 0, z > 0), n == 2))
-        def _():
-            x_copy(i, 1).start()
-
+        if diagonal:
+            stage_a(n + 1, range(parts))
+
+        @pl.when(jnp.logical_and(by_x(n + 1), jnp.logical_or(is_low, jnp.logical_not(in_plane(n + 1)))))
+        def _():
+            stage_b(n + 1)
+
+        dvw_acc[...] += dot_nn(lat_t[...], dv_s[...])
+
+        if not diagonal:
+            stage_a(n + 2, early)
+
+            @pl.when(jnp.logical_and(jnp.logical_and(x == 0, z > 0), n == 2))
+            def _():
+                for k in late:
+                    x_copy(i, k).start()
+
+    slot(jnp.int32(0), True)
+
+    def later_slot(n, carry):
+        slot(n, False)
         return carry
 
-    lax.fori_loop(0, last + 1, slot, 0)
+    lax.fori_loop(1, last + 1, later_slot, 0)
 
     @pl.when(is_low)
     def _():
         for h in range(heads):
-            fq_v[:, h * width : (h + 1) * width] = (scale * dqt_s[1, h]).T[:, :width].astype(BF16)
+            fq_v[:, h * width : (h + 1) * width] = (scale * dqt_s[1, h]).T.astype(BF16)
         back_copy().start()
 
     def wrows(k):
         return pl.ds(pl.multiple_of(k * lrows, lrows), lrows)
 
-    def dvx_copy():
-        return remote(dvw_b.at[1 - x], dvx_rx, dvxs.at[0], dvxr.at[0], x_peer)
+    def dvx_copy(d):
+        zz = (z + d) % nz
+        return remote(dvw_b.at[1 - x, zz], dvx_rx.at[zz], dvxs.at[d], dvxr.at[d], x_peer)
+
+    send_order = tuple(range(1, nz)) + (0,)
 
     def dv_copy(d):
         zz = (z + d) % nz
@@ -529,53 +541,63 @@
     for k in range(ns):
         dvw_b[k % 2, k // 2] = dvw_acc[k * lrows : (k + 1) * lrows, :].astype(BF16)
 
+    stage_r2(last)
+
+    @pl.when(last > 3)
+    def _():
+        stage_r4(last - 3)
+
+    @pl.when(last > 0)
+    def _():
+        stage_r3(last - 1)
+
+    @pl.when(x == 1)
+    def _():
+        for d in send_order:
+            dvx_copy(d).start()
+
+        @pl.when(last > 2)
+        def _():
+            stage_r4(last - 2)
+
+    @pl.when(jnp.logical_not(is_top))
+    def _():
+        for h in range(heads):
+            q_v[:, h * width : (h + 1) * width] = (
+                (scale * dqt_s[0, h]).T.astype(BF16)
+            )
+
+    stage_r3(last)
+
     @pl.when(x == 0)
     def _():
-        dvx_copy().start()
-
-    stage_r2(last)
-
-    @pl.when(last > 3)
-    def _():
-        stage_r4(last - 3)
-
-    @pl.when(last > 0)
-    def _():
-        stage_r3(last - 1)
-
-    @pl.when(x == 1)
-    def _():
-        dvx_copy().start()
-
-    @pl.when(jnp.logical_not(is_top))
-    def _():
-        for h in range(heads):
-            dq_ref[:, h * width : (h + 1) * width] = (
-                (scale * dqt_s[0, h]).T[:, :width].astype(BF16)
-            )
-
-    stage_r3(last)
+        for d in send_order:
+            dvx_copy(d).start()
 
     def tail(n, carry):
         stage_r4(n)
         return carry
 
-    lax.fori_loop(lax.max(last - 2, 1), lower + 1, tail, 0)
-    dvx_copy().wait_recv()
-    dvx_copy().wait_send()
+    lax.fori_loop(lax.max(last - 2 + x, 1), lower + 1, tail, 0)
     for d in range(1, nz):
+        dvx_copy(d).wait_recv()
         zz = (z + d) % nz
         dvw_b[x, zz] = (dvw_acc[wrows(2 * zz + x), :] + dvx_rx[zz].astype(F32)).astype(BF16)
         dv_copy(d).start()
 
     @pl.when(is_top)
     def _():
+        for k in range(4):
+            visit_copy(k).wait_send()
         back_copy().wait_recv()
         for h in range(heads):
-            dq_ref[:, h * width : (h + 1) * width] = (
-                (scale * dqt_s[0, h]).T[:, :width]
+            q_v[:, h * width : (h + 1) * width] = (
+                (scale * dqt_s[0, h]).T
                 + fq_v[:, h * width : (h + 1) * width].astype(F32)
             ).astype(BF16)
+
+    dq_out = pltpu.make_async_copy(q_v, dq_hbm, ld.at[2])
+    dq_out.start()
 
     def ag_y(d, k):
         yy = (y + d) % ny
@@ -611,6 +633,7 @@
         for d in range(1, ny):
             ag_y(d, k).start()
 
+    dvx_copy(0).wait_recv()
     dvw = dvw_acc[wrows(i), :] + dvx_rx[z].astype(F32)
     for d in range(1, nz):
         dv_wait(d).wait_recv()
@@ -640,18 +663,13 @@
 
     @pl.when(has_next)
     def _():
-        z_copy(i, 0).wait_send()
-        z_copy(i, 1).wait_send()
+        for k in range(parts):
+            z_copy(i, k).wait_send()
 
     @pl.when(jnp.logical_or(x == 0, is_low))
     def _():
-        x_copy(i, 0).wait_send()
-        x_copy(i, 1).wait_send()
-
-    @pl.when(is_top)
-    def _():
-        for k in range(4):
-            visit_copy(k).wait_send()
+        for k in range(parts):
+            x_copy(i, k).wait_send()
 
     @pl.when(is_low)
     def _():
@@ -678,6 +696,8 @@
     lax.fori_loop(1, last + 1, drain, 0)
     for d in range(1, nz):
         dv_copy(d).wait_send()
+    for d in range(nz):
+        dvx_copy(d).wait_send()
     for k in range(chunks):
         for d in range(1, ny):
             ag_y(d, k).wait_send()
@@ -685,6 +705,7 @@
     ag_c.wait_send()
     out_copy(peer_half, 1).start()
     drope_ref[...] = fin[:, latent_dim : latent_dim + ROPE].astype(F32).T
+    dq_out.wait()
     out_copy(my_half, 0).wait()
     out_copy(peer_half, 1).wait()
 
@@ -697,13 +718,14 @@
     lrows = latent_dim // ns
     ny = tp // 2
     chunks = min(4, rows // tp // 32)
+    parts = chunks
     hbm = pl.BlockSpec(memory_space=pl.ANY)
     vmem = pl.BlockSpec(memory_space=pltpu.VMEM)
     dma = pltpu.SemaphoreType.DMA
     return pl.pallas_call(
         functools.partial(fused_kernel, ns, tp, heads, latent_dim),
         in_specs=[hbm, hbm, hbm, vmem, hbm, vmem, hbm, hbm],
-        out_specs=[vmem, hbm, vmem, vmem],
+        out_specs=[hbm, hbm, vmem, vmem],
         out_shape=[
             jax.ShapeDtypeStruct(queries.shape, BF16),
             jax.ShapeDtypeStruct(latent.shape, BF16),
@@ -721,10 +743,11 @@
             pltpu.VMEM((2, heads, rows, WIDE), BF16),
             pltpu.VMEM((2, heads, WIDE, rows), BF16),
             pltpu.VMEM((2, heads, VDIM, rows), BF16),
-            pltpu.VMEM((2, heads, WIDE, rows), F32),
+            pltpu.VMEM((2, heads, NOPE + ROPE, rows), F32),
             pltpu.VMEM((2, heads, rows), F32),
             pltpu.VMEM((heads, rows, WIDE), BF16),
-            pltpu.VMEM((heads, WIDE, rows), BF16),
+            pltpu.VMEM((heads, NOPE + ROPE, rows), BF16),
+            pltpu.VMEM((latent_dim, rows), BF16),
             pltpu.VMEM((rows, hv), BF16),
             pltpu.VMEM((rows, hv), BF16),
             pltpu.VMEM((rows, hv), BF16),
@@ -740,12 +763,12 @@
             pltpu.VMEM((rows // tp, packed), F32),
             pltpu.VMEM((rows, packed), BF16),
             dma((6,)),
-            dma((ns, 2)),
-            dma((ns, 2)),
-            dma((ns, 2)),
-            dma((ns, 2)),
-            dma((ns,)),
-            dma((ns,)),
+            dma((ns, parts)),
+            dma((ns, parts)),
+            dma((ns, parts)),
+            dma((ns, parts)),
+            dma((ns, parts)),
+            dma((ns, parts)),
             dma((ns, chunks)),
             dma((ns, chunks)),
             dma((ns,)),
@@ -756,8 +779,8 @@
             dma((ns, chunks)),
             dma((ns // 2,)),
             dma((ns // 2,)),
-            dma((1,)),
-            dma((1,)),
+            dma((ns // 2,)),
+            dma((ns // 2,)),
             dma((max(ny - 1, 1), chunks)),
             dma((max(ny - 1, 1), chunks)),
             dma((1,)),
@@ -771,12 +794,41 @@
     )(queries, out_grad, attn_out, lse, latent, rope_t, key_weight, value_weight)
 
 
+def finish_kernel(dq_ref, dlat_ref, drope_ref, dvw_ref, dq_out, dlat_out, drope_out, dvw_out):
+    dq_out[...] = dq_ref[...]
+    dlat_out[...] = dlat_ref[...].astype(F32)
+    drope_out[...] = drope_ref[...]
+    dvw_out[...] = dvw_ref[...]
+
+
+def finish(dq, dlat, drope_t, dvw):
+    steps = 2
+
+    def rows_of(a):
+        return pl.BlockSpec((a.shape[0] // steps, a.shape[1]), lambda k: (k, 0))
+
+    specs = [rows_of(a) for a in (dq, dlat, drope_t, dvw)]
+    return pl.pallas_call(
+        finish_kernel,
+        grid=(steps,),
+        in_specs=specs,
+        out_specs=specs,
+        out_shape=[
+            jax.ShapeDtypeStruct(dq.shape, BF16),
+            jax.ShapeDtypeStruct(dlat.shape, F32),
+            jax.ShapeDtypeStruct(drope_t.shape, F32),
+            jax.ShapeDtypeStruct(dvw.shape, F32),
+        ],
+        compiler_params=pltpu.CompilerParams(dimension_semantics=("arbitrary",)),
+    )(dq, dlat, drope_t, dvw)
+
+
 def per_device(queries, latent, rope_key, key_weight, value_weight, log_sums, attn_out, out_grad):
     d_queries, dlat, drope_t, d_value_weight = fused_backward(
         lax.axis_size("sp"), lax.axis_size("tp"),
         queries, out_grad, attn_out, log_sums, latent, rope_key.T, key_weight, value_weight,
     )
-    d_latent = dlat.astype(F32)
+    d_queries, d_latent, drope_t, d_value_weight = finish(d_queries, dlat, drope_t, d_value_weight)
     d_rope = drope_t.T
     return (d_queries, d_latent, d_rope, d_value_weight)
 

time: 111 us -> 101 us (0.910); the launches traced: 108 us -> 101 us
  Pallas kernels: 103 us -> 99.9 us
  other arithmetic: 2.88 us -> 0 us
  local copies, waits for them, and re-layouts: 2.25 us -> 0 us
    pallas_call x1, Pallas kernels: 103 us -> 96.9 us  [fused_backward(): pl.pallas_call(functools.partial(fused_kernel, ns, tp, heads, latent_dim)...]
    pallas_call x0 -> x1, Pallas kernels: none -> 3.02 us  [finish(): pl.pallas_call(finish_kernel, grid=(steps,), in_specs=specs, out_specs=sp...]
    convert_element_type x1 -> x0, other arithmetic: 2.88 us -> none  [per_device(): d_latent = dlat.astype(F32)]
    unnamed x9 -> x0, local copies, waits for them, and re-layouts: 2.25 us -> none
where the time goes in v5:
time: 101 us
  Pallas kernels  99.9 us (99%)
    pallas_call x1, Pallas kernels, fused_backward(): pl.pallas_call(functools.partial(fused_kernel, ns, tp, heads, latent_dim)...  96.9 us
    pallas_call x1, Pallas kernels, finish(): pl.pallas_call(finish_kernel, grid=(steps,), in_specs=specs, out_specs=sp...  3.02 us

profile of v5, /device:TPU:0, one launch (start us, length us, event | category | flops | bytes accessed | tf_op | source)
XLA Modules:
  0.0 100.6 jit_solution(2012933848279991750)
XLA Ops:
  0.6 96.9 %shard_map.111 = (bf16[512,768]{1,0:T(8,128)(2,1)}, bf16[512,1024]{1,0:T(8,128)(2,1)}, f32[64,512]{1,0:T(8,128)}, f32[128,512]{1,0:T(8,128)}) custom-call(bf16[512,768]{1,0:T(8,128)(2,1)} %q_hbm.1, bf16[512,512]{1,0:T(8,128)(2,1)} %g_hbm.1, bf16[512,512]{1,0:T(8,128)(2,1)} %ao_hbm.1, f32[4,512]{1,0:T(4,128)} %lse_ref.1, bf16[512,1024]{1,0:T(8,128)(2,1)} %lat_hbm.1, ...), custom_call_target="tpu_custom_call" | custom-call | tf_op jit(solution)/shard_map/pallas_call | solution.py:725
  97.5 3.0 %shard_map.112 = (bf16[512,768]{1,0:T(8,128)(2,1)}, f32[512,1024]{1,0:T(8,128)}, f32[64,512]{1,0:T(8,128)}, f32[128,512]{1,0:T(8,128)}) custom-call(bf16[512,768]{1,0:T(8,128)(2,1)} %get-tuple-element.12.dq_ref, bf16[512,1024]{1,0:T(8,128)(2,1)} %get-tuple-element.13.dlat_ref, f32[64,512]{1,0:T(8,128)} %get-tuple-element.14.drope_ref, ...), custom_call_target="tpu_custom_call" | custom-call | tf_op jit(solution)/shard_map/pallas_call | solution.py:811

commit v6 on v5

--- a/solution.py
+++ b/solution.py
@@ -40,8 +40,8 @@
     wv_hbm,
     dq_hbm,
     dlat_hbm,
-    drope_ref,
-    dvw_ref,
+    drope_hbm,
+    dvw_hbm,
     q_v,
     g_v,
     fq_v,
@@ -71,6 +71,8 @@
     orx,
     own_acc,
     fin,
+    dvw_o,
+    drope_o,
     ld,
     zr,
     zs,
@@ -194,14 +196,18 @@
     def bit_of(j, k):
         return lat_rows(j, pl.multiple_of(c * half + k * bit, bit), bit)
 
+    def pair_of(j):
+        return lax.select(j // 2 == z, jnp.int32(2), (z + nz - 1 - j // 2) % 2)
+
     def z_copy(j, k):
-        return remote(bit_of(j, k), bit_of(j, k), zs.at[j, k], zr.at[j, k], above)
+        return remote(bit_of(j, k), bit_of(j, k), zs.at[pair_of(j), k], zr.at[j // 2, k], above)
 
     def x_copy(j, k):
-        return remote(bit_of(j, k), bit_of(j, k), xs.at[j, k], xr.at[j, k], x_peer)
-
-    def c_copy(j, k):
-        return remote(bit_of(j, k), bit_of(j, k), cs.at[j, k], cr.at[j, k], core_peer)
+        return remote(bit_of(j, k), bit_of(j, k), xs.at[pair_of(j), k], xr.at[j // 2, k], x_peer)
+
+    def c_copy(n, k):
+        j = block_of(n)
+        return remote(bit_of(j, k), bit_of(j, k), cs.at[n % 4, k], cr.at[n % 4, k], core_peer)
 
     has_next = z + 1 < nz
 
@@ -241,7 +247,7 @@
             for k in pieces:
                 z_copy(j, k).wait_recv()
                 x_copy(j, k).start()
-                c_copy(j, k).start()
+                c_copy(n, k).start()
 
                 @pl.when(goes_on(n))
                 def _():
@@ -251,7 +257,7 @@
         j = block_of(n)
         for k in range(parts):
             x_copy(j, k).wait_recv()
-            c_copy(j, k).start()
+            c_copy(n, k).start()
 
     def sends_done(n):
         j = block_of(n)
@@ -259,7 +265,7 @@
         @pl.when(jnp.logical_or(own_column(n), by_x(n)))
         def _():
             for k in range(parts):
-                c_copy(j, k).wait_send()
+                c_copy(n, k).wait_send()
 
         @pl.when(own_column(n))
         def _():
@@ -288,30 +294,32 @@
         yy = (y + d) % ny
         return remote(
             lat_all.at[part_of(n), rows_of(yy, k)], yrx.at[j, d - 1, chunk(k)],
-            ys.at[j, d - 1, k], yr.at[j, d - 1, k], {"sp": i, "tp": yy * 2 + c},
+            ys.at[n % 4, d - 1, k], yr.at[n % 4, d - 1, k], {"sp": i, "tp": yy * 2 + c},
         )
 
     def xr_copy(n, k):
         j = block_of(n)
         return remote(
-            lat_all.at[part_of(n), rows_of(y, k)], xrx.at[j, chunk(k)], xrs.at[j, k], xrr.at[j, k], x_peer
+            lat_all.at[part_of(n), rows_of(y, k)], xrx.at[j, chunk(k)], xrs.at[j // 2, k],
+            xrr.at[j // 2, k], x_peer,
         )
 
     def o_copy(n, k):
         return remote(
-            lat_all.at[part_of(n), rows_of(y, k)], orx.at[z, chunk(k)], ors.at[key_of(n), k], orr.at[z, k],
+            lat_all.at[part_of(n), rows_of(y, k)], orx.at[z, chunk(k)], ors.at[block_of(n) // 2, k],
+            orr.at[z, k],
             {"sp": block_of(n), "tp": t},
         )
 
     def v_copy(n, k):
         return remote(
-            lat_all.at[part_of(n), rows_of(y, k)], orx.at[nz, chunk(k)], ors.at[key_of(n), k],
+            lat_all.at[part_of(n), rows_of(y, k)], orx.at[nz, chunk(k)], ors.at[1, k],
             orr.at[nz, k], x_peer,
         )
 
     def o_wait(zz, k):
         return remote(
-            lat_all.at[i, rows_of(y, k)], orx.at[zz, chunk(k)], ors.at[i, k], orr.at[zz, k], x_peer
+            lat_all.at[i, rows_of(y, k)], orx.at[zz, chunk(k)], ors.at[0, k], orr.at[zz, k], x_peer
         )
 
     def stage_r2(n):
@@ -426,7 +434,7 @@
             @pl.when(jnp.logical_or(own_column(n), by_x(n)))
             def _():
                 for k in range(parts):
-                    c_copy(j, k).wait_recv()
+                    c_copy(n, k).wait_recv()
 
             @pl.when(n == base + 1)
             def _():
@@ -556,9 +564,9 @@
         for d in send_order:
             dvx_copy(d).start()
 
-        @pl.when(last > 2)
-        def _():
-            stage_r4(last - 2)
+    @pl.when(jnp.logical_and(x == 1, last > 2))
+    def _():
+        stage_r4(last - 2)
 
     @pl.when(jnp.logical_not(is_top))
     def _():
@@ -633,12 +641,6 @@
         for d in range(1, ny):
             ag_y(d, k).start()
 
-    dvx_copy(0).wait_recv()
-    dvw = dvw_acc[wrows(i), :] + dvx_rx[z].astype(F32)
-    for d in range(1, nz):
-        dv_wait(d).wait_recv()
-        dvw = dvw + dvw_rx[d].astype(F32)
-    dvw_ref[...] = dvw
     for k in range(chunks):
         for d in range(1, ny):
             ag_y_wait(d, k).wait_recv()
@@ -656,6 +658,14 @@
         )
 
     out_copy(my_half, 0).start()
+    dvx_copy(0).wait_recv()
+    dvw = dvw_acc[wrows(i), :] + dvx_rx[z].astype(F32)
+    for d in range(1, nz):
+        dv_wait(d).wait_recv()
+        dvw = dvw + dvw_rx[d].astype(F32)
+    dvw_o[...] = dvw
+    dvw_out = pltpu.make_async_copy(dvw_o, dvw_hbm, ld.at[3])
+    dvw_out.start()
 
     @pl.when(last > 0)
     def _():
@@ -702,12 +712,17 @@
         for d in range(1, ny):
             ag_y(d, k).wait_send()
     ag_c_wait.wait_recv()
+    out_copy(peer_half, 1).start()
+    drope_o[...] = fin[:, latent_dim : latent_dim + ROPE].astype(F32).T
+    drope_out = pltpu.make_async_copy(drope_o, drope_hbm, ld.at[4])
+    drope_out.start()
     ag_c.wait_send()
-    out_copy(peer_half, 1).start()
-    drope_ref[...] = fin[:, latent_dim : latent_dim + ROPE].astype(F32).T
-    dq_out.wait()
-    out_copy(my_half, 0).wait()
-    out_copy(peer_half, 1).wait()
+    with jax.named_scope("outs"):
+        dq_out.wait()
+        dvw_out.wait()
+        out_copy(my_half, 0).wait()
+        out_copy(peer_half, 1).wait()
+        drope_out.wait()
 
 
 def fused_backward(ns, tp, queries, out_grad, attn_out, lse, latent, rope_t, key_weight, value_weight):
@@ -725,7 +740,7 @@
     return pl.pallas_call(
         functools.partial(fused_kernel, ns, tp, heads, latent_dim),
         in_specs=[hbm, hbm, hbm, vmem, hbm, vmem, hbm, hbm],
-        out_specs=[hbm, hbm, vmem, vmem],
+        out_specs=[hbm, hbm, hbm, hbm],
         out_shape=[
             jax.ShapeDtypeStruct(queries.shape, BF16),
             jax.ShapeDtypeStruct(latent.shape, BF16),
@@ -762,21 +777,23 @@
             pltpu.VMEM((ns // 2 + 1, rows // tp, packed), BF16),
             pltpu.VMEM((rows // tp, packed), F32),
             pltpu.VMEM((rows, packed), BF16),
+            pltpu.VMEM((lrows, hv), F32),
+            pltpu.VMEM(rope_t.shape, F32),
             dma((6,)),
-            dma((ns, parts)),
-            dma((ns, parts)),
-            dma((ns, parts)),
-            dma((ns, parts)),
-            dma((ns, parts)),
-            dma((ns, parts)),
-            dma((ns, chunks)),
-            dma((ns, chunks)),
+            dma((ns // 2, parts)),
+            dma((3, parts)),
+            dma((ns // 2, parts)),
+            dma((3, parts)),
+            dma((4, parts)),
+            dma((4, parts)),
+            dma((ns // 2, chunks)),
+            dma((ns // 2, chunks)),
             dma((ns,)),
             dma((ns,)),
-            dma((ns, max(ny - 1, 1), chunks)),
-            dma((ns, max(ny - 1, 1), chunks)),
+            dma((4, max(ny - 1, 1), chunks)),
+            dma((4, max(ny - 1, 1), chunks)),
             dma((ns // 2 + 1, chunks)),
-            dma((ns, chunks)),
+            dma((ns // 2, chunks)),
             dma((ns // 2,)),
             dma((ns // 2,)),
             dma((ns // 2,)),

time: 101 us -> 98.5 us (0.975)
  Pallas kernels: 99.9 us -> 96.8 us
    pallas_call x1, Pallas kernels: 96.9 us -> 93.8 us  [fused_backward(): pl.pallas_call(functools.partial(fused_kernel, ns, tp, heads, latent_dim)...]
where the time goes in v6:
time: 98.5 us; the launch traced here: 97.5 us
  Pallas kernels  96.8 us (98%)
    pallas_call x1, Pallas kernels, fused_backward(): pl.pallas_call(functools.partial(fused_kernel, ns, tp, heads, latent_dim)...  93.8 us
    pallas_call x1, Pallas kernels, finish(): pl.pallas_call(finish_kernel, grid=(steps,), in_specs=specs, out_specs=sp...  3.02 us

profile of v6, /device:TPU:0, one launch (start us, length us, event | category | flops | bytes accessed | tf_op | source)
XLA Modules:
  0.0 97.5 jit_solution(8168420323573078061)
XLA Ops:
  0.6 93.8 %shard_map.111 = (bf16[512,768]{1,0:T(8,128)(2,1)}, bf16[512,1024]{1,0:T(8,128)(2,1)}, f32[64,512]{1,0:T(8,128)}, f32[128,512]{1,0:T(8,128)}) custom-call(bf16[512,768]{1,0:T(8,128)(2,1)} %q_hbm.1, bf16[512,512]{1,0:T(8,128)(2,1)} %g_hbm.1, bf16[512,512]{1,0:T(8,128)(2,1)} %ao_hbm.1, f32[4,512]{1,0:T(4,128)} %lse_ref.1, bf16[512,1024]{1,0:T(8,128)(2,1)} %lat_hbm.1, ...), custom_call_target="tpu_custom_call" | custom-call | tf_op jit(solution)/shard_map/pallas_call | solution.py:740
  94.4 3.0 %shard_map.112 = (bf16[512,768]{1,0:T(8,128)(2,1)}, f32[512,1024]{1,0:T(8,128)}, f32[64,512]{1,0:T(8,128)}, f32[128,512]{1,0:T(8,128)}) custom-call(bf16[512,768]{1,0:T(8,128)(2,1)} %get-tuple-element.12.dq_ref, bf16[512,1024]{1,0:T(8,128)(2,1)} %get-tuple-element.13.dlat_ref, f32[64,512]{1,0:T(8,128)} %get-tuple-element.14.drope_ref, ...), custom_call_target="tpu_custom_call" | custom-call | tf_op jit(solution)/shard_map/pallas_call | solution.py:828

commit v7 on v6

--- a/solution.py
+++ b/solution.py
@@ -641,16 +641,19 @@
         for d in range(1, ny):
             ag_y(d, k).start()
 
-    for k in range(chunks):
-        for d in range(1, ny):
+    def ag_c(d):
+        at = pl.ds(pl.multiple_of(c * half + (y + ny - d) % ny * piece, piece), piece)
+        return remote(fin.at[at], fin.at[at], acs.at[d], acr.at[d], core_peer)
+
+    def ag_c_wait(d):
+        at = pl.ds(pl.multiple_of((1 - c) * half + (y + ny - d) % ny * piece, piece), piece)
+        return remote(fin.at[at], fin.at[at], acs.at[d], acr.at[d], core_peer)
+
+    ag_c(0).start()
+    for d in range(1, ny):
+        for k in range(chunks):
             ag_y_wait(d, k).wait_recv()
-    ag_c = remote(
-        fin.at[pl.ds(my_half, half)], fin.at[pl.ds(my_half, half)], acs.at[0], acr.at[0], core_peer
-    )
-    ag_c_wait = remote(
-        fin.at[pl.ds(peer_half, half)], fin.at[pl.ds(peer_half, half)], acs.at[0], acr.at[0], core_peer
-    )
-    ag_c.start()
+        ag_c(d).start()
 
     def out_copy(at, k):
         return pltpu.make_async_copy(
@@ -711,12 +714,14 @@
     for k in range(chunks):
         for d in range(1, ny):
             ag_y(d, k).wait_send()
-    ag_c_wait.wait_recv()
+    for d in range(ny):
+        ag_c_wait(d).wait_recv()
     out_copy(peer_half, 1).start()
     drope_o[...] = fin[:, latent_dim : latent_dim + ROPE].astype(F32).T
     drope_out = pltpu.make_async_copy(drope_o, drope_hbm, ld.at[4])
     drope_out.start()
-    ag_c.wait_send()
+    for d in range(ny):
+        ag_c(d).wait_send()
     with jax.named_scope("outs"):
         dq_out.wait()
         dvw_out.wait()
@@ -800,8 +805,8 @@
             dma((ns // 2,)),
             dma((max(ny - 1, 1), chunks)),
             dma((max(ny - 1, 1), chunks)),
-            dma((1,)),
-            dma((1,)),
+            dma((ny,)),
+            dma((ny,)),
             dma((5,)),
             dma((5,)),
         ],

time: 98.5 us -> 98.1 us (level)
  no operation moved by 1% of the time
where the time goes in v7:
time: 98.1 us; the launch traced here: 97.1 us
  Pallas kernels  96.4 us (98%)
    pallas_call x1, Pallas kernels, fused_backward(): pl.pallas_call(functools.partial(fused_kernel, ns, tp, heads, latent_dim)...  93.4 us
    pallas_call x1, Pallas kernels, finish(): pl.pallas_call(finish_kernel, grid=(steps,), in_specs=specs, out_specs=sp...  3.02 us

profile of v7, /device:TPU:0, one launch (start us, length us, event | category | flops | bytes accessed | tf_op | source)
XLA Modules:
  0.0 97.1 jit_solution(6123996463855172301)
XLA Ops:
  0.6 93.4 %shard_map.111 = (bf16[512,768]{1,0:T(8,128)(2,1)}, bf16[512,1024]{1,0:T(8,128)(2,1)}, f32[64,512]{1,0:T(8,128)}, f32[128,512]{1,0:T(8,128)}) custom-call(bf16[512,768]{1,0:T(8,128)(2,1)} %q_hbm.1, bf16[512,512]{1,0:T(8,128)(2,1)} %g_hbm.1, bf16[512,512]{1,0:T(8,128)(2,1)} %ao_hbm.1, f32[4,512]{1,0:T(4,128)} %lse_ref.1, bf16[512,1024]{1,0:T(8,128)(2,1)} %lat_hbm.1, ...), custom_call_target="tpu_custom_call" | custom-call | tf_op jit(solution)/shard_map/pallas_call | solution.py:745
  94.0 3.0 %shard_map.112 = (bf16[512,768]{1,0:T(8,128)(2,1)}, f32[512,1024]{1,0:T(8,128)}, f32[64,512]{1,0:T(8,128)}, f32[128,512]{1,0:T(8,128)}) custom-call(bf16[512,768]{1,0:T(8,128)(2,1)} %get-tuple-element.12.dq_ref, bf16[512,1024]{1,0:T(8,128)(2,1)} %get-tuple-element.13.dlat_ref, f32[64,512]{1,0:T(8,128)} %get-tuple-element.14.drope_ref, ...), custom_call_target="tpu_custom_call" | custom-call | tf_op jit(solution)/shard_map/pallas_call | solution.py:833
